TPU v7x, 512 devices: a whole 4x8x8 slice. The times are simulated.
512 devices in a mesh: ep: 32 (over z, x), tp: 16 (over y, core).
Axes of the slice: x: 4, y: 8, z: 8, core: 2. Of those that a mesh axis runs over, the one named last changes fastest.
Arguments:
- mixer_tokens: bfloat16 [6144, 2048], P('ep'), may hold values from -6 to 6
- mixer_gain: float32 [2048], replicated, may hold values from 0.1 to 1.9
- query_weight: bfloat16 [1024, 2048], P('tp'), may hold values from -1 to 1
- key_weight: bfloat16 [1024, 2048], P('tp'), may hold values from -1 to 1
- value_weight: bfloat16 [1024, 2048], P('tp'), may hold values from -0.125 to 0.125
- forget_weight: bfloat16 [2048, 16], P(None, 'tp'), may hold values from -0.125 to 0.125
- forget_bias: float32 [32, 16], P('ep', 'tp'), may hold values from 2.98 to 10.4
- output_weight: bfloat16 [1024, 2048], P(None, 'tp'), may hold values from -0.1875 to 0.1875
- expert_tokens: bfloat16 [4096, 2048], P('ep'), may hold values from -6 to 6
- expert_gain: float32 [2048], replicated, may hold values from 0.1 to 1.9
- routes: int32 [4096, 2], P('ep'), may hold values from 0 to 31, all different within a row; in each aligned block of 128 rows (0 to 127, 128 to 255, ...) at most 16 rows name the same one
- route_weights: float32 [4096, 2], P('ep'), may hold values from 0.2 to 1
- gate_weight: bfloat16 [32, 3584, 2048], P('ep', 'tp'), may hold values from -0.125 to 0.125
- up_weight: bfloat16 [32, 3584, 2048], P('ep', 'tp'), may hold values from -0.125 to 0.125
- down_weight: bfloat16 [32, 3584, 2048], P('ep', 'tp'), may hold values from -0.09375 to 0.09375
Outputs:
- mixer_output: bfloat16 [6144, 2048], P('ep', 'tp')
- expert_output: bfloat16 [4096, 2048], P('ep', 'tp')
Inputs may be any that keep to these rules, and one draw needn't show every extreme that they name: `routes`: within the tokens of one index of ep (aligned blocks of 128 rows) no expert is named more than 16 times, a bound that some block reaches; the 2 experts of a token differ.
All inputs are finite; a program needn't handle non-finite values.
Results may differ from a plain program's by a relative error of at most 0.019.
Values may be sent and summed in bfloat16 or wider, within the bound.
A program may use at most 128 MiB of HBM per device.

v0:
```python
import jax
import jax.numpy as jnp
from jax import lax
from jax.sharding import Mesh
from jax.sharding import PartitionSpec as P

HD = 64
TP = ("tp_0", "tp_1")


MEAN_FLOOR = 0.1
HEAD_FLOOR = 1.0
START_MAX = -1e30


def copy_for_each(array, axis):
    copies = jnp.broadcast_to(array, (lax.axis_size(axis), *array.shape))
    return lax.all_to_all(copies, axis, split_axis=0, concat_axis=0, tiled=True)


def laid_out(parts, dim):
    parts = jnp.moveaxis(parts, 0, dim)
    lengths = parts.shape
    return parts.reshape(*lengths[:dim], lengths[dim] * lengths[dim + 1], *lengths[dim + 2 :])


def collect(array, axis, dim):
    parts = copy_for_each(array, axis)
    return laid_out(parts, dim)


def in_one_piece(arrays, axis, dim, along):
    ends, at = ([], 0)
    for a in arrays[:-1]:
        at += a.shape[along]
        ends.append(at)
    both = jnp.concatenate(arrays, axis=along)
    return tuple(jnp.split(lax.all_gather(both, axis, axis=dim, tiled=True), ends, axis=along))


def split_up(array, dim, peers):
    before, after = (array.shape[:dim], array.shape[dim + 1 :])
    return jnp.moveaxis(array.reshape(*before, peers, -1, *after), dim, 0)


def sum_by_chip(array, chips, core, dim):
    sizes = (lax.axis_size(chips), lax.axis_size(core))
    parts = split_up(array, dim, sizes[0] * sizes[1])
    inside = parts.shape[1:]
    parts = parts.reshape(*sizes, *inside).swapaxes(0, 1).reshape(-1, *inside)
    parts = lax.psum_scatter(parts, core, scatter_dimension=0, tiled=True)
    return lax.psum_scatter(parts, chips, scatter_dimension=0, tiled=True)[0]


def normed_rows(inputs, gain):
    values = inputs.astype(jnp.float32)
    square = jnp.mean(values * values, axis=-1, keepdims=True)
    return (values * lax.rsqrt(jnp.maximum(square, MEAN_FLOOR)) * gain).astype(jnp.bfloat16)


def by_rows(left, weight):
    return lax.dot_general(
        left, weight, (((1,), (1,)), ((), ())), preferred_element_type=jnp.float32
    )


def on_device(
    mixer_tokens,
    mixer_gain,
    query_weight,
    key_weight,
    value_weight,
    forget_weight,
    forget_bias,
    output_weight,
    expert_tokens,
    expert_gain,
    routes,
    route_weights,
    gate_weight,
    up_weight,
    down_weight,
):
    row_count = mixer_tokens.shape[0]
    feature_count = mixer_tokens.shape[1]
    local_heads = forget_weight.shape[1]
    normed = normed_rows(mixer_tokens, mixer_gain)
    queries = by_rows(normed, query_weight).astype(jnp.bfloat16)
    key_rows = by_rows(normed, key_weight).astype(jnp.bfloat16)
    value_rows = by_rows(normed, value_weight).astype(jnp.bfloat16)
    pre_gate = jnp.dot(normed, forget_weight, preferred_element_type=jnp.float32) + forget_bias
    log_gates = jax.nn.log_sigmoid(pre_gate)
    all_gates = collect(log_gates, "ep", 0)
    cumulative = jnp.cumsum(all_gates, axis=0)
    offset = lax.axis_index("ep") * row_count
    query_cum = lax.dynamic_slice_in_dim(cumulative, offset, row_count, 0)
    head_query = queries.reshape(row_count, local_heads, HD)
    query_pos = offset + jnp.arange(row_count, dtype=jnp.int32)
    initial = (
        jnp.full((local_heads, row_count), START_MAX, jnp.float32),
        jnp.zeros((row_count, local_heads, HD), jnp.float32),
    )
    pieces = in_one_piece((key_rows, value_rows), "ep", 0, 1)

    def compute(current):
        running, accumulated = current
        piece_keys, piece_values = pieces
        key_count = piece_keys.shape[0]
        scores = jnp.einsum(
            "qhd,khd->hqk",
            head_query,
            piece_keys.reshape(key_count, local_heads, HD),
            preferred_element_type=jnp.float32,
        ) * HD ** (-0.5)
        scores = scores + query_cum.T[:, :, None] - cumulative.T[:, None, :]
        key_pos = jnp.arange(key_count, dtype=jnp.int32)
        scores = jnp.where(key_pos[None, None, :] <= query_pos[None, :, None], scores, -jnp.inf)
        new_max = jnp.maximum(running, jnp.max(scores, axis=-1))
        weights = jnp.exp(scores - new_max[:, :, None]).astype(jnp.bfloat16)
        update = jnp.einsum(
            "hqk,khd->qhd",
            weights,
            piece_values.reshape(key_count, local_heads, HD),
            preferred_element_type=jnp.float32,
        )
        factor = jnp.exp(running - new_max).T[:, :, None]
        return (new_max, accumulated * factor + update)

    running, accumulated = lax.cond(
        jnp.int32(0) < offset + row_count, compute, lambda current: current, initial
    )
    rescale = lax.rsqrt(jnp.mean(accumulated * accumulated, axis=-1, keepdims=True) + HEAD_FLOOR)
    head_out = (accumulated * rescale).reshape(row_count, local_heads * HD).astype(jnp.bfloat16)
    mixer_output = jnp.dot(
        lax.all_gather(head_out, TP, axis=1, tiled=True),
        output_weight,
        preferred_element_type=jnp.float32,
    ).astype(jnp.bfloat16)
    expert_normed = normed_rows(expert_tokens, expert_gain)
    token_count, top_count = routes.shape
    experts = lax.axis_size("ep")
    capacity = 2 * top_count * token_count // experts
    flat_routes = routes.reshape(-1)
    onehot = (flat_routes[:, None] == jnp.arange(experts, dtype=jnp.int32)[None, :]).astype(
        jnp.int32
    )
    slot_rank = jnp.sum((jnp.cumsum(onehot, axis=0) - 1) * onehot, axis=1)
    slot_index = flat_routes * capacity + slot_rank
    slot_owner = jnp.full((experts * capacity,), token_count, jnp.int32)
    slot_owner = slot_owner.at[slot_index].set(
        jnp.arange(token_count * top_count, dtype=jnp.int32) // top_count
    )
    padded = jnp.concatenate([expert_normed, jnp.zeros((1, feature_count), jnp.bfloat16)], axis=0)
    outgoing = padded[slot_owner].reshape(experts, capacity, feature_count)
    slots = lax.all_to_all(outgoing, "ep", split_axis=0, concat_axis=0, tiled=True)
    sources, slot_count, _ = slots.shape
    flat_rows = slots.reshape(sources * slot_count, feature_count)
    gate_act = by_rows(flat_rows, gate_weight[0])
    up_act = by_rows(flat_rows, up_weight[0])
    hidden = (jax.nn.silu(gate_act) * up_act).astype(jnp.bfloat16)
    partial_value = jnp.dot(hidden, down_weight[0], preferred_element_type=jnp.float32)
    partial_value = partial_value.reshape(sources, slot_count, feature_count)
    summed = (
        sum_by_chip(partial_value.astype(jnp.bfloat16), "tp_0", "tp_1", 2)
        .astype(jnp.float32)
        .astype(jnp.bfloat16)
    )
    returned = lax.all_to_all(summed, "ep", split_axis=0, concat_axis=0, tiled=True)
    gathered = returned.reshape(experts * capacity, returned.shape[2])[slot_index]
    weighted = gathered.astype(jnp.float32) * route_weights.reshape(-1)[:, None]
    expert_output = jnp.sum(weighted.reshape(token_count, top_count, returned.shape[2]), axis=1)
    return (mixer_output, expert_output.astype(jnp.bfloat16))


def solution(mesh):
    split = Mesh(mesh.devices.reshape(mesh.shape["ep"], 8, 2), ("ep", "tp_0", "tp_1"))
    return jax.shard_map(
        on_device,
        mesh=split,
        in_specs=(
            P("ep", None),
            P(),
            P(TP, None),
            P(TP, None),
            P(TP, None),
            P(None, TP),
            P("ep", TP),
            P(None, TP),
            P("ep", None),
            P(),
            P("ep", None),
            P("ep", None),
            P("ep", TP, None),
            P("ep", TP, None),
            P("ep", TP, None),
        ),
        out_specs=(P("ep", TP), P("ep", TP)),
        check_vma=False,
    )
```

profile of v0, /device:TPU:1, one launch (start us, length us, event | category | flops | bytes accessed | tf_op | source)
XLA Modules:
  0.0 213.0 jit_solution(6719221904024799314)
XLA Ops:
  8.1 0.9 copy.34
  11.1 1.4 scatter_custom_fusion
  12.5 1.2 fusion.20
  13.8 1.2 fusion.22
  15.0 3.3 %gather_fusion = bf16[512,2048]{1,0:T(8,128)(2,1)} fusion(bf16[129,2048]{1,0:T(8,128)(2,1)S(1)} %concatenate.7, s32[1024]{0:T(1024)S(1)} %pad_clamp_fusion.1), kind=kCustom, calls=%fused_computation | custom fusion | bytes 4196352 | tf_op jit(solution)/shard_map/gather | solution.py:154
  18.4 62.5 %all_to_all.15 = bf16[32,16,2048]{2,1,0:T(8,128)(2,1)S(1)} all-to-all(bf16[32,16,2048]{2,1,0:T(8,128)(2,1)} %bitcast.82), channel_id=1, replica_groups=mesh['ep'=32,'tp_0'=8,'tp_1'=2] {'ep'}, dimensions={0} | all-to-all | bytes 4194304 | tf_op jit(solution)/shard_map/all_to_all | solution.py:155
  80.9 0.8 fusion.25
  82.1 0.8 fusion.19
  83.0 0.7 convolution_convert_fusion
  84.4 1.9 copy.38
  86.4 1.0 copy-done.2
  88.6 0.7 copy.31
  89.4 15.1 %reduce-scatter.3.cloned.1.call-done = bf16[8,32,16,128]{3,2,1,0:T(8,128)(2,1)} async-done(((bf16[16,32,16,128]{3,2,1,0:T(8,128)(2,1)}), bf16[8,32,16,128]{3,2,1,0:T(8,128)(2,1)}) %reduce-scatter.3.cloned.1.call-update) | async-done | bytes 1048592 | tf_op jit(solution)/shard_map/reduce_scatter | solution.py:51
  106.3 9.5 %all-to-all-start = ((f32[32,192,1]{1,2,0:T(1,128)}), f32[32,192,1]{1,2,0:T(1,128)S(1)}, u32[]{:S(2)}, u32[]{:S(2)}) async-start(f32[32,192,1]{1,2,0:T(1,128)} %broadcast_in_dim.38), calls=%async_computation | async-start | bytes 65536 | tf_op jit(solution)/shard_map/all_to_all | solution.py:18
  116.4 7.9 %all-to-all-done = f32[32,192,1]{1,2,0:T(1,128)S(1)} async-done(((f32[32,192,1]{1,2,0:T(1,128)}), f32[32,192,1]{1,2,0:T(1,128)S(1)}, u32[]{:S(2)}, u32[]{:S(2)}) %all-to-all-start) | async-done | bytes 24608 | tf_op jit(solution)/shard_map/all_to_all | solution.py:18
  125.2 43.9 %all-gather.3.cloned.1.call-done = bf16[6144,128]{1,0:T(8,128)(2,1)} async-done(((bf16[192,128]{1,0:T(8,128)(2,1)}), bf16[6144,128]{1,0:T(8,128)(2,1)}) %all-gather.3.cloned.1.call-update) | async-done | bytes 1572880 | tf_op jit(solution)/shard_map/all_gather | solution.py:38
  169.1 5.2 %conditional.1 = (f32[192,1,64]{0,2,1:T(8,128)S(1)}, f32[192,1,1]{0,2,1:T(1,128)S(1)}) conditional(s32[]{:T(128)} %convert_element_type.62, () %tuple.24, (s32[]{:T(128)}, s32[192]{0:T(256)S(1)}, bf16[6144,128]{1,0:T(8,128)(2,1)}, bf16[192,64]{0,1:T(8,128)(2,1)S(1)}, f32[1,48,128]{2,1,0:T(8,128)S(1)}, /*index=5*/f32[1,49]{1,0:T(1,128)S(1)}) %tuple.25), branch_computations={%region_3.4_spmd, %region_4.7_spmd} | conditional | flops 311470656 | bytes 19058006 | solution.py:129
  169.3 3.2 %fusion.40 = (f32[192]{0:T(256)S(1)}, f32[192,6144]{1,0:T(8,128)S(1)}) fusion(f32[6144]{0:T(1024)S(1)} %bitcast_add_fusion, f32[192]{0:T(256)S(1)} %bitcast.98, bf16[192,64]{0,1:T(8,128)(2,1)S(1)} %get-tuple-element.117, bf16[6144,128]{1,0:T(8,128)(2,1)} %get-tuple-element.93, s32[192]{0:T(256)S(1)} %broadcast_add_fusion), kind=kOutput, calls=%fused_computation.75 | convolution fusion | flops 158072640 | bytes 6342912 | tf_op jit(solution)/shard_map/cond/branch_1_fun/qhd,khd->hqk/dot_general | solution.py:109
  172.6 1.7 multiply_reduce_fusion
  174.3 4.9 %all-to-all-start.2 = ((bf16[32,16,128]{2,1,0:T(8,128)(2,1)}), bf16[32,16,128]{2,1,0:T(8,128)(2,1)S(1)}, u32[]{:S(2)}, u32[]{:S(2)}) async-start(bf16[32,16,128]{2,1,0:T(8,128)(2,1)} %bitcast.92), calls=%async_computation.4 | async-start | bytes 262144 | tf_op jit(solution)/shard_map/all_to_all | solution.py:168
  179.3 23.6 %all-gather = bf16[192,1,1024]{0,2,1:T(8,128)(2,1)S(1)} all-gather(bf16[192,1,64]{0,2,1:T(8,128)(2,1)S(1)} %multiply_convert_fusion), channel_id=2, replica_groups=mesh['ep'=32,'tp_0'=8,'tp_1'=2] {'tp_0','tp_1'}, dimensions={2}, use_global_device_ids=true | all-gather | bytes 417792 | tf_op jit(solution)/shard_map/all_gather | solution.py:135
  202.9 0.9 convolution_convert_fusion.1
  203.8 0.9 gather_fusion.1
  204.7 0.9 fusion.28
  (75 shorter events, 7.4 us)
Async XLA Ops:
  8.0 75.0 %copy-start = (bf16[1,224,2048]{2,1,0:T(8,128)(2,1)S(1)}, bf16[1,224,2048]{2,1,0:T(8,128)(2,1)}, u32[]{:S(2)}) copy-start(bf16[1,224,2048]{2,1,0:T(8,128)(2,1)} %param.31) | copy-start | bytes 2752516
  8.0 96.5 %reduce-scatter.3.cloned.1.call-start = ((), (), s32[]{:S(2)}) async-start(), calls=%async_computation.6 | async-start | bytes 3145728 | tf_op jit(solution)/shard_map/reduce_scatter | solution.py:51
  18.4 62.5 %copy-start.5 = (bf16[1,224,2048]{2,1,0:T(8,128)(2,1)S(1)}, bf16[1,224,2048]{2,1,0:T(8,128)(2,1)}, u32[]{:S(2)}) copy-start(bf16[1,224,2048]{2,1,0:T(8,128)(2,1)} %param.29) | copy-start | bytes 2752516
  80.9 1.2 copy-start.6
  86.3 1.1 copy-start.2
  86.3 1.4 copy-start.7
  86.3 1.4 copy-start.11
  86.3 1.8 copy-start.8
  86.3 82.8 %all-gather.3.cloned.1.call-start = ((), (), s32[]{:S(2)}) async-start(), calls=%async_computation.5 | async-start | bytes 1622016 | tf_op jit(solution)/shard_map/all_gather | solution.py:38
  87.7 17.5 %copy-start.10 = (bf16[2048,1]{0,1:T(2,128)(2,1)S(1)}, bf16[2048,1]{0,1:T(2,128)(2,1)}, u32[]{:S(2)}) copy-start(bf16[2048,1]{0,1:T(2,128)(2,1)} %param.22) | copy-start | bytes 12292
  88.1 27.7 %copy-start.9 = (bf16[64,2048]{1,0:T(8,128)(2,1)S(1)}, bf16[64,2048]{1,0:T(8,128)(2,1)}, u32[]{:S(2)}) copy-start(bf16[64,2048]{1,0:T(8,128)(2,1)} %param.19) | copy-start | bytes 786436
  89.4 85.0 %reduce-scatter.5.cloned.1.call-start = ((), (), s32[]{:S(2)}) async-start(), calls=%async_computation.7 | async-start | bytes 1179648 | tf_op jit(solution)/shard_map/reduce_scatter | solution.py:52
  104.6 11.8 %copy-start.4 = (f32[128,2]{0,1:T(2,128)S(1)}, f32[128,2]{0,1:T(2,128)}, u32[]{:S(2)}) copy-start(f32[128,2]{0,1:T(2,128)} %param.28) | copy-start | bytes 3076
  106.3 18.0 %all-to-all-start = ((f32[32,192,1]{1,2,0:T(1,128)}), f32[32,192,1]{1,2,0:T(1,128)S(1)}, u32[]{:S(2)}, u32[]{:S(2)}) async-start(f32[32,192,1]{1,2,0:T(1,128)} %broadcast_in_dim.38), calls=%async_computation | async-start | bytes 65536 | tf_op jit(solution)/shard_map/all_to_all | solution.py:18
  169.1 33.8 %copy-start.3 = (bf16[1024,128]{1,0:T(8,128)(2,1)S(1)}, bf16[1024,128]{1,0:T(8,128)(2,1)}, u32[]{:S(2)}) copy-start(bf16[1024,128]{1,0:T(8,128)(2,1)} %param.24) | copy-start | bytes 786436
  169.3 3.3 %copy-start.1 = (bf16[6144,128]{1,0:T(8,128)(2,1)S(1)}, bf16[6144,128]{1,0:T(8,128)(2,1)}, u32[]{:S(2)}) copy-start(bf16[6144,128]{1,0:T(8,128)(2,1)} %get-tuple-element.93) | copy-start | bytes 4718596 | tf_op jit(solution)/shard_map/cond
  174.3 29.5 %all-to-all-start.2 = ((bf16[32,16,128]{2,1,0:T(8,128)(2,1)}), bf16[32,16,128]{2,1,0:T(8,128)(2,1)S(1)}, u32[]{:S(2)}, u32[]{:S(2)}) async-start(bf16[32,16,128]{2,1,0:T(8,128)(2,1)} %bitcast.92), calls=%async_computation.4 | async-start | bytes 262144 | tf_op jit(solution)/shard_map/all_to_all | solution.py:168
Sparse Core Ops, SparseCore 0:
  86.4 18.0 reduce-scatter.2
  107.4 37.7 reduce-scatter.4
Sparse Core Ops, SparseCore 1:
  90.5 78.5 all-gather.2
where the time goes:
time: 213 us
  blocking collectives  86.1 us (40%)
  waiting for transfers between devices  67 us (31%)
  between operations  16.4 us (8%)
  starting transfers between devices  14.6 us (7%)
  local copies, waits for them, and re-layouts  13.1 us (6%)
  matrix products  9.89 us (5%)
  other arithmetic  5.83 us (3%)
    all_to_all x1, blocking collectives, on_device(): lax.all_to_all(outgoing, 'ep', split_axis=0, concat_axis=0, tiled=True)  62.5 us
    all_gather x1, waiting for transfers between devices, in_one_piece(): lax.all_gather(both, axis, axis=dim, tiled=True)  43.9 us
    all_gather x1, blocking collectives, on_device(): lax.all_gather(head_out, TP, axis=1, tiled=True)  23.6 us
    reduce_scatter x1, waiting for transfers between devices, sum_by_chip(): parts = lax.psum_scatter(parts, core, scatter_dimension=0, tiled=True)  15.1 us
    all_to_all x1, starting transfers between devices, copy_for_each(): return lax.all_to_all(copies, axis, split_axis=0, concat_axis=0, tiled=True)  9.54 us
    all_to_all x1, waiting for transfers between devices, copy_for_each(): return lax.all_to_all(copies, axis, split_axis=0, concat_axis=0, tiled=True)  7.9 us
    all_to_all x1, starting transfers between devices, on_device(): lax.all_to_all(summed, 'ep', split_axis=0, concat_axis=0, tiled=True)  4.92 us
  transfers between devices with their start and end apart: 5, of which 3 were waited for; matrix products, arithmetic and copies ran while one was open for 5% of the time, Pallas kernels for 0%

commit v1 on v0

v1 whole, which is shorter than its diff:
```python
import jax
import jax.numpy as jnp
from jax import lax
from jax.experimental import pallas as pl
from jax.experimental.pallas import tpu as pltpu
from jax.sharding import Mesh
from jax.sharding import PartitionSpec as P

NZ, NX, NY, NC = 8, 4, 8, 2
HD = 64
ROWS_A = 192
ROWS_B = 128
D = 2048
FF = 224
CAP = 16
SLOTS = NZ * NX * CAP
QUART = 256
MEAN_FLOOR = 0.1
HEAD_FLOOR = 1.0
LOW = -1e30
MESH = pl.DeviceIdType.MESH
TP = ("y", "c")
EP = ("z", "x")
NEAR = (0, 1, 7, 2, 6, 3, 5, 4)
f32, bf16 = jnp.float32, jnp.bfloat16


def by_rows(left, right):
    return lax.dot_general(left, right, (((1,), (1,)), ((), ())), preferred_element_type=f32)


def exact(left, right):
    return jnp.dot(left, right, precision=lax.Precision.HIGHEST, preferred_element_type=f32)


def iota(shape, dim):
    return lax.broadcasted_iota(jnp.int32, shape, dim)


def rcopy(src, dst, send, recv, **where):
    return pltpu.make_async_remote_copy(
        src_ref=src,
        dst_ref=dst,
        send_sem=send,
        recv_sem=recv,
        device_id=where,
        device_id_type=MESH,
    )


def kernel(
    mt, mg, qw, kw, vw, fw, fb, ow, et, eg, rt, rw, gw_h, uw_h, dw_h,
    mo, eo,
    gw, uw, dw, dwp, w4, an, en, outrows, dispatch, comb,
    xm, xo, gacc, uacc, hid, hidp, pb, sbp, sbm, rbp, rbm, fin, res,
    qbuf, kvbuf, gmb, gx, gadj, gz, bias, po, pr, hbm, hbo, bw,
    lsem, ssem, dsem, ysem, psem, rsp, rsm, msem,
):
    z, x, y, c = (lax.axis_index(n) for n in ("z", "x", "y", "c"))
    other = 1 - c

    local = [
        pltpu.make_async_copy(gw_h.at[0], gw, lsem.at[0]),
        pltpu.make_async_copy(uw_h.at[0], uw, lsem.at[1]),
        pltpu.make_async_copy(dw_h.at[0], dw, lsem.at[2]),
        pltpu.make_async_copy(kw, w4.at[pl.ds(0, HD)], lsem.at[3]),
        pltpu.make_async_copy(vw, w4.at[pl.ds(HD, HD)], lsem.at[4]),
        pltpu.make_async_copy(qw, w4.at[pl.ds(2 * HD, HD)], lsem.at[5]),
    ]
    for cp in local:
        cp.start()

    barrier = pltpu.get_barrier_semaphore()
    for dz in range(NZ):
        for dx in range(NX):
            if dz or dx:
                pl.semaphore_signal(
                    barrier,
                    inc=1,
                    device_id={"z": lax.rem(z + dz, NZ), "x": lax.rem(x + dx, NX)},
                    device_id_type=MESH,
                )
    for dy in range(1, NY):
        pl.semaphore_signal(
            barrier, inc=1, device_id={"y": lax.rem(y + dy, NY)}, device_id_type=MESH
        )
    pl.semaphore_signal(barrier, inc=1, device_id={"c": other}, device_id_type=MESH)

    lane0 = pl.multiple_of((lax.rem(y, 4) * 2 + c) * QUART, QUART)

    def norm_b(i, _):
        rows = pl.ds(pl.multiple_of(i * 16, 16), 16)
        v = et[rows, :].astype(f32)
        sq = jnp.mean(v * v, axis=-1, keepdims=True)
        part = et[rows, pl.ds(lane0, QUART)].astype(f32)
        scaled = part * lax.rsqrt(jnp.maximum(sq, MEAN_FLOOR)) * eg[:, pl.ds(lane0, QUART)]
        en[rows, :] = scaled.astype(bf16)
        return 0

    lax.fori_loop(0, ROWS_B // 16, norm_b, 0)

    eid = iota((32, ROWS_B), 0)
    first = (eid == rt[0:1, :]).astype(f32)
    second = (eid == rt[1:2, :]).astype(f32)
    named = first + second
    before = (iota((ROWS_B, ROWS_B), 0) < iota((ROWS_B, ROWS_B), 1)).astype(bf16)
    rank = jnp.dot(named.astype(bf16), before, preferred_element_type=f32)
    rank = jnp.where(named > 0.5, rank, -1.0)
    pick = (lax.div(iota((SLOTS, 32), 0), CAP) == iota((SLOTS, 32), 1)).astype(f32)
    wide = jnp.dot(pick.astype(bf16), rank.astype(bf16), preferred_element_type=f32)
    chosen = wide == lax.rem(iota((SLOTS, ROWS_B), 0), CAP).astype(f32)
    dispatch[...] = chosen.astype(f32).astype(bf16)
    outrows[...] = jnp.dot(dispatch[...], en[...], preferred_element_type=f32).astype(bf16)

    pl.semaphore_wait(barrier, NZ * NX - 1 + NY - 1 + 1)

    local[2].wait()
    dwcopy = rcopy(dw, dwp, ssem.at[0], msem.at[0], c=other)
    dwcopy.start()
    mine = pl.multiple_of((z * NX + x) * CAP, CAP)
    for p, dzs in enumerate(NEAR):
        for dxs in range(NX):
            if dzs == 0 and dxs == 0:
                continue
            zt, xt = lax.rem(z + (NZ - dzs), NZ), lax.rem(x + (NX - dxs), NX)
            rcopy(
                outrows.at[pl.ds(pl.multiple_of((zt * NX + xt) * CAP, CAP), CAP)],
                xm.at[0, pl.ds((p * NX + dxs) * CAP, CAP)],
                ssem.at[1],
                dsem.at[p // 2],
                z=zt,
                x=xt,
            ).start()
    xm[0, 0:CAP, :] = outrows[pl.ds(mine, CAP), :]

    def norm_a(i, _):
        rows = pl.ds(pl.multiple_of(i * 16, 16), 16)
        v = mt[rows, :].astype(f32)
        sq = jnp.mean(v * v, axis=-1, keepdims=True)
        an[rows, :] = (v * lax.rsqrt(jnp.maximum(sq, MEAN_FLOOR)) * mg[...]).astype(bf16)
        return 0

    lax.fori_loop(0, ROWS_A // 16, norm_a, 0)
    w4[3 * HD : 4 * HD, :] = jnp.zeros((HD, D), bf16)
    for cp in local[3:6]:
        cp.wait()
    kvbuf[0:ROWS_A, :] = by_rows(an[...], w4[0 : 2 * HD, :]).astype(bf16)
    qs = by_rows(an[...], w4[2 * HD : 4 * HD, :]).astype(bf16) * jnp.asarray(HD**-0.5, bf16)
    qbuf[0:ROWS_A, :] = qs
    pre = by_rows(fw[...], an[...]) + fb[...]
    log_gate = jnp.minimum(pre, 0.0) - jnp.log1p(jnp.exp(-jnp.abs(pre)))
    upto = (iota((ROWS_A, 256), 0) <= iota((ROWS_A, 256), 1)).astype(f32)
    gmb[...] = exact(jnp.broadcast_to(log_gate, (8, ROWS_A)), upto)
    for dx in range(1, NX):
        xt = lax.rem(x + dx, NX)
        rcopy(gmb, gx.at[NX - dx], ssem.at[2], msem.at[1], x=xt).start()
        rcopy(
            qbuf.at[pl.ds(0, ROWS_A)],
            qbuf.at[pl.ds((NX - dx) * ROWS_A, ROWS_A)],
            ssem.at[3],
            msem.at[2],
            x=xt,
        ).start()
    for dz in range(1, NZ):
        rcopy(
            kvbuf.at[pl.ds(0, ROWS_A)],
            kvbuf.at[pl.ds((NZ - dz) * ROWS_A, ROWS_A)],
            ssem.at[4],
            msem.at[3],
            z=lax.rem(z + dz, NZ),
        ).start()
    gx0 = gx.at[pl.ds(1, NX - 1)]
    rcopy(gx0, gx0, ssem.at[2], msem.at[1], x=x).wait_recv()
    ahead = jnp.zeros((8, 1), f32)
    total = gmb[:, 255:256]
    for k in range(1, NX):
        t = gx[k, :, 255:256]
        ahead = ahead + t * (lax.rem(x + k, NX) < x).astype(f32)
        total = total + t
    gadj[...] = jnp.where(iota((8, 256), 1) < ROWS_A, gmb[...] + ahead, total)
    for dz in range(1, NZ):
        rcopy(gadj, gz.at[NZ - dz], ssem.at[5], msem.at[4], z=lax.rem(z + dz, NZ)).start()

    up, down = lax.rem(y + 1, NY), lax.rem(y + NY - 1, NY)
    up2, down2 = lax.rem(y + 2, NY), lax.rem(y + NY - 2, NY)
    for g in range(4):
        skip = CAP if g == 0 else 0
        got = xm.at[0, pl.ds(g * 128 + skip, 128 - skip)]
        rcopy(got, got, ssem.at[1], dsem.at[g], c=other).wait_recv()
        piece = pl.ds(g * 128, 128)
        src = xm.at[0, piece]
        rcopy(src, xm.at[3, piece], ssem.at[6], ysem.at[3], y=up).start()
        rcopy(src, xm.at[1, piece], ssem.at[7], ysem.at[1], y=down).start()
        rcopy(src, xm.at[2, piece], ssem.at[8], ysem.at[2], y=up2 if g < 2 else down2).start()
        rcopy(src, xo.at[0, piece], ssem.at[9], psem.at[0], c=other).start()

    weights = first * rw[0:1, :] + second * rw[1:2, :]
    spread = exact(pick, weights)
    comb[...] = jnp.where(dispatch[...] > 0.5, spread, 0.0).T
    bw[...] = jnp.zeros_like(bw)
    for h in range(16):
        bw[h * 128 : h * 128 + HD, 0:128] = ow[h * HD : (h + 1) * HD, :]
        bw[h * 128 + HD : h * 128 + 128, 128:256] = ow[h * HD : (h + 1) * HD, :]

    gz0 = gz.at[pl.ds(1, NZ - 1)]
    rcopy(gz0, gz0, ssem.at[5], msem.at[4], z=z).wait_recv()
    bias[...] = jnp.full((8, NZ * ROWS_A), LOW, f32)
    bias[:, 0:ROWS_A] = -gadj[:, 0:ROWS_A]
    back = jnp.zeros((8, 1), f32)
    for k in range(1, NZ):
        at = NZ - k
        back = back + gz[at, :, 255:256]
        bias[:, at * ROWS_A : (at + 1) * ROWS_A] = jnp.where(
            z - k >= 0, back - gz[at, :, 0:ROWS_A], LOW
        )
    q0 = qbuf.at[pl.ds(0, 3 * ROWS_A)]
    rcopy(q0, q0, ssem.at[3], msem.at[2], x=x).wait_recv()
    kv0 = kvbuf.at[pl.ds(0, 7 * ROWS_A)]
    rcopy(kv0, kv0, ssem.at[4], msem.at[3], z=z).wait_recv()
    HALF = ROWS_A // 2

    def attend(i, _):
        rows = pl.ds(pl.multiple_of(i * HALF, 32), HALF)
        dx = lax.div(i, 2)
        delta = (lax.rem(x + dx, NX) - x) * ROWS_A + lax.rem(i, 2) * HALF
        scores = by_rows(qbuf[rows, :], kvbuf[...]) + bias[0:1, :]
        lane = iota((HALF, 256), 1)
        seen = (lane <= iota((HALF, 256), 0) + delta) | (lane >= ROWS_A)
        scores = jnp.concatenate(
            [jnp.where(seen, scores[:, :256], LOW), scores[:, 256:]], axis=1
        )
        top = jnp.max(scores, axis=-1, keepdims=True)
        weight = jnp.exp(scores - top).astype(bf16)
        out = jnp.dot(weight, kvbuf[...], preferred_element_type=f32)
        po[rows, :] = jnp.where(iota((HALF, 128), 1) < HD, top, out)
        return 0

    lax.fori_loop(0, 2 * NX, attend, 0)
    for dx in range(1, NX):
        rcopy(
            po.at[pl.ds(dx * ROWS_A, ROWS_A)],
            pr.at[pl.ds((NX - dx) * ROWS_A, ROWS_A)],
            ssem.at[10],
            msem.at[5],
            x=lax.rem(x + dx, NX),
        ).start()

    local[0].wait()
    local[1].wait()

    def product(rows, k, core, start):
        cols = pl.ds(pl.multiple_of((lax.rem(y + k, 4) * 2 + core) * QUART, QUART), QUART)
        g, u = by_rows(rows, gw[:, cols]), by_rows(rows, uw[:, cols])
        if start:
            gacc[...], uacc[...] = g, u
        else:
            gacc[...] += g
            uacc[...] += u

    product(xm[0], 0, c, True)
    for k in (1, 3, 2):
        rcopy(xm.at[k], xm.at[k], ssem.at[6], ysem.at[k], y=up).wait_recv()
        rcopy(xm.at[k], xo.at[k], ssem.at[10 + k], psem.at[k], c=other).start()
        product(xm[k], k, c, False)
    for k in (0, 1, 3, 2):
        rcopy(xo.at[k], xo.at[k], ssem.at[9], psem.at[k], c=other).wait_recv()
        product(xo[k], k, other, False)
    gate = gacc[...]
    hid[...] = (gate * jax.nn.sigmoid(gate) * uacc[...]).astype(bf16)
    hcopy = rcopy(hid, hidp, ssem.at[14], msem.at[6], c=other)
    hcopy.start()
    dwcopy.wait_recv()
    hcopy.wait_recv()

    def down_block(j):
        cols = pl.ds(pl.multiple_of((lax.rem(y + j, NY) * 2 + c) * 128, 128), 128)
        pb[j] = jnp.dot(hid[...], dw[:, cols], preferred_element_type=f32) + jnp.dot(
            hidp[...], dwp[:, cols], preferred_element_type=f32
        )

    def plus(d, q, received):
        rows = pl.ds(q * 128, 128)
        v = pb[d, rows, :]
        if received:
            slot = rbp.at[d, rows]
            rcopy(slot, slot, ssem.at[15], rsp.at[d, q], y=up).wait_recv()
            v = v + rbp[d, rows, :].astype(f32)
        held = pl.ds(d * SLOTS + q * 128, 128)
        sbp[held, :] = v.astype(bf16)
        rcopy(
            sbp.at[held], rbp.at[d - 1, rows], ssem.at[15], rsp.at[d - 1, q], y=up
        ).start()

    def minus(d, q, received):
        rows = pl.ds(q * 128, 128)
        v = pb[NY - d, rows, :]
        if received:
            slot = rbm.at[d, rows]
            rcopy(slot, slot, ssem.at[16], rsm.at[d, q], y=down).wait_recv()
            v = v + rbm[d, rows, :].astype(f32)
        held = pl.ds(d * SLOTS + q * 128, 128)
        sbm[held, :] = v.astype(bf16)
        rcopy(
            sbm.at[held], rbm.at[d - 1, rows], ssem.at[16], rsm.at[d - 1, q], y=down
        ).start()

    down_block(4)
    for q in (0, 1):
        plus(4, q, False)
        minus(4, q + 2, False)
    down_block(3)
    down_block(5)
    for q in (0, 1):
        plus(3, q + 2, False)
        minus(3, q, False)
    for j in (2, 6, 1, 7, 0):
        down_block(j)
    for q in (0, 1):
        plus(3, q, True)
        minus(3, q + 2, True)
    for d in (2, 1):
        for q in (2, 3, 0, 1):
            plus(d, q, True)
            minus(d, (q + 2) % 4, True)

    pr0 = pr.at[pl.ds(0, 3 * ROWS_A)]
    rcopy(pr0, pr0, ssem.at[10], msem.at[5], x=x).wait_recv()
    parts = [po[0:ROWS_A, :]] + [pr[k * ROWS_A : (k + 1) * ROWS_A, :] for k in range(1, NX)]
    tops = [p[:, 0:1] for p in parts]
    top = jnp.maximum(jnp.maximum(tops[0], tops[1]), jnp.maximum(tops[2], tops[3]))
    att = sum(p * jnp.exp(t - top) for p, t in zip(parts, tops))
    att = jnp.where(iota((ROWS_A, 128), 1) < HD, 0.0, att)
    mean = jnp.sum(att * att, axis=-1, keepdims=True) * (1.0 / HD)
    head = att * lax.rsqrt(mean + HEAD_FLOOR)
    packed = jnp.where(
        iota((HALF, 128), 1) < HD, pltpu.roll(head[:HALF], HD, 1), head[HALF:]
    )
    hbm[pl.ds(y, 1)] = packed.astype(bf16)[None]
    for dy in range(1, NY):
        rcopy(hbm.at[y], hbm.at[y], ssem.at[17], msem.at[7], y=lax.rem(y + dy, NY)).start()

    for q in (0, 2, 1, 3):
        rows = pl.ds(q * 128, 128)
        ps, ms = rbp.at[0, rows], rbm.at[0, rows]
        rcopy(ps, ps, ssem.at[15], rsp.at[0, q], y=up).wait_recv()
        rcopy(ms, ms, ssem.at[16], rsm.at[0, q], y=down).wait_recv()
        v = pb[0, rows, :] + rbp[0, rows, :].astype(f32) + rbm[0, rows, :].astype(f32)
        fin[rows, :] = v.astype(bf16)
        for p in (2 * q, 2 * q + 1):
            for dxs in range(NX):
                at = pl.ds((p * NX + dxs) * CAP, CAP)
                if p == 0 and dxs == 0:
                    res[pl.ds(mine, CAP), :] = fin[0:CAP, :]
                    continue
                rcopy(
                    fin.at[at],
                    res.at[pl.ds(mine, CAP)],
                    ssem.at[18],
                    msem.at[8],
                    z=lax.rem(z + NEAR[p], NZ),
                    x=lax.rem(x + dxs, NX),
                ).start()

    h0 = hbm.at[pl.ds(0, NY - 1)]
    rcopy(h0, h0, ssem.at[17], msem.at[7], y=up).wait_recv()
    hc = rcopy(hbm, hbo, ssem.at[19], msem.at[9], c=other)
    hc.start()
    acc = jnp.zeros((HALF, 256), f32)
    for k in range(NY):
        acc = acc + jnp.dot(
            hbm[k], bw[pl.ds(pl.multiple_of((2 * k + c) * 128, 128), 128), :],
            preferred_element_type=f32,
        )
    hc.wait_recv()
    for k in range(NY):
        acc = acc + jnp.dot(
            hbo[k], bw[pl.ds(pl.multiple_of((2 * k + other) * 128, 128), 128), :],
            preferred_element_type=f32,
        )
    mo[0:HALF, :] = acc[:, 0:128].astype(bf16)
    mo[HALF:ROWS_A, :] = acc[:, 128:256].astype(bf16)

    r0 = res.at[pl.ds(0, SLOTS - CAP)]
    rcopy(r0, r0, ssem.at[18], msem.at[8], z=z).wait_recv()
    eo[...] = exact(comb[...], res[...].astype(f32)).astype(bf16)

    def sent(ref, sem):
        rcopy(ref, ref, ssem.at[sem], msem.at[0], c=other).wait_send()

    sent(dw, 0)
    sent(outrows.at[pl.ds(0, SLOTS - CAP)], 1)
    sent(gx.at[pl.ds(0, 3)], 2)
    sent(q0, 3)
    sent(kv0, 4)
    sent(gz0, 5)
    for s in (6, 7, 8, 9):
        sent(xm.at[0], s)
    sent(pr0, 10)
    for s in (11, 12, 13):
        sent(xm.at[0], s)
    sent(hid, 14)
    for s in (15, 16):
        sent(sbp.at[pl.ds(0, 14 * 128)], s)
    sent(h0, 17)
    sent(r0, 18)
    sent(hbm, 19)


def on_device(mt, mg, qw, kw, vw, fw, fb, ow, et, eg, rt, rw, gw, uw, dw):
    vmem = pl.BlockSpec(memory_space=pltpu.VMEM)
    hbm = pl.BlockSpec(memory_space=pl.ANY)
    dma = pltpu.SemaphoreType.DMA
    return pl.pallas_call(
        kernel,
        name="mixer_and_experts",
        out_shape=(
            jax.ShapeDtypeStruct((ROWS_A, 128), bf16),
            jax.ShapeDtypeStruct((ROWS_B, 128), bf16),
        ),
        in_specs=[vmem, vmem, hbm, hbm, hbm, vmem, vmem, vmem, vmem, vmem, vmem, vmem]
        + [hbm] * 3,
        out_specs=(vmem, vmem),
        scratch_shapes=[
            pltpu.VMEM((FF, D), bf16),
            pltpu.VMEM((FF, D), bf16),
            pltpu.VMEM((FF, D), bf16),
            pltpu.VMEM((FF, D), bf16),
            pltpu.VMEM((4 * HD, D), bf16),
            pltpu.VMEM((ROWS_A, D), bf16),
            pltpu.VMEM((ROWS_B, QUART), bf16),
            pltpu.VMEM((SLOTS, QUART), bf16),
            pltpu.VMEM((SLOTS, ROWS_B), bf16),
            pltpu.VMEM((ROWS_B, SLOTS), f32),
            pltpu.VMEM((4, SLOTS, QUART), bf16),
            pltpu.VMEM((4, SLOTS, QUART), bf16),
            pltpu.VMEM((SLOTS, FF), f32),
            pltpu.VMEM((SLOTS, FF), f32),
            pltpu.VMEM((SLOTS, FF), bf16),
            pltpu.VMEM((SLOTS, FF), bf16),
            pltpu.VMEM((NY, SLOTS, 128), f32),
            pltpu.VMEM((5 * SLOTS, 128), bf16),
            pltpu.VMEM((5 * SLOTS, 128), bf16),
            pltpu.VMEM((4, SLOTS, 128), bf16),
            pltpu.VMEM((4, SLOTS, 128), bf16),
            pltpu.VMEM((SLOTS, 128), bf16),
            pltpu.VMEM((SLOTS, 128), bf16),
            pltpu.VMEM((NX * ROWS_A, 128), bf16),
            pltpu.VMEM((NZ * ROWS_A, 128), bf16),
            pltpu.VMEM((8, 256), f32),
            pltpu.VMEM((NX, 8, 256), f32),
            pltpu.VMEM((8, 256), f32),
            pltpu.VMEM((NZ, 8, 256), f32),
            pltpu.VMEM((8, NZ * ROWS_A), f32),
            pltpu.VMEM((NX * ROWS_A, 128), f32),
            pltpu.VMEM((NX * ROWS_A, 128), f32),
            pltpu.VMEM((NY, ROWS_A // 2, 128), bf16),
            pltpu.VMEM((NY, ROWS_A // 2, 128), bf16),
            pltpu.VMEM((D, 256), bf16),
            dma((6,)),
            dma((20,)),
            dma((4,)),
            dma((4,)),
            dma((4,)),
            dma((4, 4)),
            dma((4, 4)),
            dma((10,)),
        ],
        compiler_params=pltpu.CompilerParams(collective_id=0, has_side_effects=True),
        cost_estimate=pl.CostEstimate(
            flops=3_000_000_000, bytes_accessed=6_000_000, transcendentals=1_200_000
        ),
    )(
        mt, mg.reshape(1, D), qw, kw, vw, fw.T, fb, ow, et, eg.reshape(1, D), rt.T, rw.T,
        gw, uw, dw,
    )


def solution(mesh):
    split = Mesh(mesh.devices.reshape(NZ, NX, NY, NC), ("z", "x", "y", "c"))
    return jax.shard_map(
        on_device,
        mesh=split,
        in_specs=(
            P(EP, None),
            P(),
            P(TP, None),
            P(TP, None),
            P(TP, None),
            P(None, TP),
            P(EP, TP),
            P(None, TP),
            P(EP, None),
            P(),
            P(EP, None),
            P(EP, None),
            P(EP, TP, None),
            P(EP, TP, None),
            P(EP, TP, None),
        ),
        out_specs=(P(EP, TP), P(EP, TP)),
        check_vma=False,
    )
```

time: 213 us -> 70.1 us (0.33)
  blocking collectives: 86.1 us -> 0 us
  waiting for transfers between devices: 67 us -> 0 us
  Pallas kernels: 0 us -> 66.6 us
  between operations: 16.4 us -> 1.3 us
  starting transfers between devices: 14.6 us -> 0 us
  local copies, waits for them, and re-layouts: 13.1 us -> 2.05 us
  matrix products: 9.89 us -> 0 us
  other arithmetic: 5.83 us -> 0 us
    pallas_call x0 -> x1, Pallas kernels: none -> 66.6 us  [on_device(): pl.pallas_call(kernel, name='mixer_and_experts', out_shape=(jax.ShapeDtyp...]
    all_to_all x1 -> x0, blocking collectives: 62.5 us -> none  [on_device(): lax.all_to_all(outgoing, 'ep', split_axis=0, concat_axis=0, tiled=True)]
    all_gather x1 -> x0, waiting for transfers between devices: 43.9 us -> none  [in_one_piece(): lax.all_gather(both, axis, axis=dim, tiled=True)]
    all_gather x1 -> x0, blocking collectives: 23.6 us -> none  [on_device(): lax.all_gather(head_out, TP, axis=1, tiled=True)]
    reduce_scatter x2 -> x0, waiting for transfers between devices: 15.2 us -> none  [the longest x1 15.1 us: sum_by_chip(): parts = lax.psum_scatter(parts, core, scatter_dimension=0, tiled=True)]
    all_to_all x2 -> x0, starting transfers between devices: 14.5 us -> none  [the longest x1 9.54 us: copy_for_each(): return lax.all_to_all(copies, axis, split_axis=0, concat_axis=0, tiled=True)]
    dot_general x10 -> x0, matrix products: 9.89 us -> none  [the longest x1 3.24 us: compute(): jnp.einsum('qhd,khd->hqk', head_query, piece_keys.reshape(key_count, loca...]
    all_to_all x2 -> x0, waiting for transfers between devices: 7.9 us -> none  [the longest x1 7.9 us: copy_for_each(): return lax.all_to_all(copies, axis, split_axis=0, concat_axis=0, tiled=True)]
  transfers between devices with their start and end apart: 5 -> 0, of which waited for: 3 -> 0; matrix products, arithmetic and copies ran while one was open for 5% -> 0% of each run, Pallas kernels for 0% -> 0%
where the time goes in v1:
time: 70.1 us; the launch traced here: 69.9 us
  Pallas kernels  66.6 us (95%)
  local copies, waits for them, and re-layouts  2.05 us (3%)
  between operations  1.3 us (2%)
    pallas_call x1, Pallas kernels, on_device(): pl.pallas_call(kernel, name='mixer_and_experts', out_shape=(jax.ShapeDtyp...  66.6 us
    unnamed x4, local copies, waits for them, and re-layouts  2.05 us

profile of v1, /device:TPU:1, one launch (start us, length us, event | category | flops | bytes accessed | tf_op | source)
XLA Modules:
  0.0 69.9 jit_solution(10702966404957530573)
XLA Ops:
  1.3 66.6 %mixer_and_experts.1 = (bf16[192,128]{1,0:T(8,128)(2,1)}, bf16[128,128]{1,0:T(8,128)(2,1)}) custom-call(bf16[192,2048]{1,0:T(8,128)(2,1)} %mt.1, f32[1,2048]{1,0:T(1,128)} %bitcast.5, bf16[64,2048]{1,0:T(8,128)(2,1)} %qw.1, bf16[64,2048]{1,0:T(8,128)(2,1)} %kw.1, bf16[64,2048]{1,0:T(8,128)(2,1)} %vw.1, bf16[1,2048]{1,0:T(2,128)(2,1)} %bitcast.6, ...), custom_call_target="tpu_custom_call" | custom-call | flops 3000000000 | bytes 6000000 | tf_op jit(solution)/shard_map/mixer_and_experts/pallas_call | solution.py:413
  67.8 0.0 copy-start
  67.8 1.4 %copy.20 = bf16[192,128]{1,0:T(8,128)(2,1)} copy(bf16[192,128]{1,0:T(8,128)(2,1)} %get-tuple-element.4) | data formatting | bytes 98304
  69.3 0.0 copy-done
  69.3 0.6 copy.21
Async XLA Ops:
  67.8 1.4 %copy-start = (bf16[128,128]{1,0:T(8,128)(2,1)S(1)}, bf16[128,128]{1,0:T(8,128)(2,1)}, u32[]{:S(2)}) copy-start(bf16[128,128]{1,0:T(8,128)(2,1)} %get-tuple-element.5) | copy-start | bytes 98308

commit v2 on v1

v2 whole, which is shorter than its diff:
```python
import jax
import jax.numpy as jnp
from jax import lax
from jax.experimental import pallas as pl
from jax.experimental.pallas import tpu as pltpu
from jax.sharding import Mesh
from jax.sharding import PartitionSpec as P

NZ, NX, NY, NC = 8, 4, 8, 2
HD = 64
ROWS_A = 192
ROWS_B = 128
D = 2048
FF = 224
CAP = 16
SLOTS = NZ * NX * CAP
QUART = 256
MEAN_FLOOR = 0.1
HEAD_FLOOR = 1.0
LOW = -1e30
MESH = pl.DeviceIdType.MESH
TP = ("y", "c")
EP = ("z", "x")
NEAR = (0, 1, 7, 2, 6, 3, 5, 4)
f32, bf16 = jnp.float32, jnp.bfloat16


def by_rows(left, right):
    return lax.dot_general(left, right, (((1,), (1,)), ((), ())), preferred_element_type=f32)


def exact(left, right):
    return jnp.dot(left, right, precision=lax.Precision.HIGHEST, preferred_element_type=f32)


def iota(shape, dim):
    return lax.broadcasted_iota(jnp.int32, shape, dim)


def rcopy(src, dst, send, recv, **where):
    return pltpu.make_async_remote_copy(
        src_ref=src,
        dst_ref=dst,
        send_sem=send,
        recv_sem=recv,
        device_id=where,
        device_id_type=MESH,
    )


def kernel(
    mt_h, mg_h, qw_h, kw_h, vw_h, fw_h, fb, ow_h, et_h, eg_h, rt_h, rw_h, gw_h, uw_h, dw_h,
    mo, eo,
    mt, mg, fw, ow, et, eg, rt, rw,
    gw, uw, dw, dwp, w4, an, en, outrows, dispatch, comb,
    xm, xo, gacc, uacc, hid, hidp, pb, sbp, sbm, rbp, rbm, fin, res,
    qbuf, kvbuf, gmb, gx, gadj, gz, bias, po, pr, hbm, hbo, bw,
    lsem, ssem, dsem, ysem, psem, rsp, rsm, msem,
):
    z, x, y, c = (lax.axis_index(n) for n in ("z", "x", "y", "c"))
    other = 1 - c

    local = [
        pltpu.make_async_copy(src, dst, lsem.at[i])
        for i, (src, dst) in enumerate(
            (
                (et_h, et),
                (eg_h, eg),
                (rt_h, rt),
                (rw_h, rw),
                (mt_h, mt),
                (mg_h, mg),
                (kw_h, w4.at[pl.ds(0, HD)]),
                (vw_h, w4.at[pl.ds(HD, HD)]),
                (qw_h, w4.at[pl.ds(2 * HD, HD)]),
                (fw_h, fw),
                (dw_h.at[0], dw),
                (gw_h.at[0], gw),
                (uw_h.at[0], uw),
                (ow_h, ow),
            )
        )
    ]
    for cp in local[:4]:
        cp.start()

    barrier = pltpu.get_barrier_semaphore()
    for dz in range(NZ):
        for dx in range(NX):
            if dz or dx:
                pl.semaphore_signal(
                    barrier,
                    inc=1,
                    device_id={"z": lax.rem(z + dz, NZ), "x": lax.rem(x + dx, NX)},
                    device_id_type=MESH,
                )
    for dy in range(1, NY):
        pl.semaphore_signal(
            barrier, inc=1, device_id={"y": lax.rem(y + dy, NY)}, device_id_type=MESH
        )
    pl.semaphore_signal(barrier, inc=1, device_id={"c": other}, device_id_type=MESH)
    for cp in local[4:]:
        cp.start()

    eid = iota((32, ROWS_B), 0)
    before = (iota((ROWS_B, ROWS_B), 0) < iota((ROWS_B, ROWS_B), 1)).astype(bf16)
    pick = (lax.div(iota((SLOTS, 32), 0), CAP) == iota((SLOTS, 32), 1)).astype(f32)
    for cp in local[:4]:
        cp.wait()
    first = (eid == rt[0:1, :]).astype(f32)
    second = (eid == rt[1:2, :]).astype(f32)
    named = first + second
    rank = jnp.dot(named.astype(bf16), before, preferred_element_type=f32)
    rank = jnp.where(named > 0.5, rank, -1.0)
    wide = jnp.dot(pick.astype(bf16), rank.astype(bf16), preferred_element_type=f32)
    chosen = wide == lax.rem(iota((SLOTS, ROWS_B), 0), CAP).astype(f32)
    dispatch[...] = chosen.astype(f32).astype(bf16)
    lane0 = pl.multiple_of((lax.rem(y, 4) * 2 + c) * QUART, QUART)

    def norm_b(i, _):
        rows = pl.ds(pl.multiple_of(i * 16, 16), 16)
        v = et[rows, :].astype(f32)
        sq = jnp.mean(v * v, axis=-1, keepdims=True)
        part = et[rows, pl.ds(lane0, QUART)].astype(f32)
        scaled = part * lax.rsqrt(jnp.maximum(sq, MEAN_FLOOR)) * eg[:, pl.ds(lane0, QUART)]
        en[rows, :] = scaled.astype(bf16)
        return 0

    lax.fori_loop(0, ROWS_B // 16, norm_b, 0, unroll=4)
    outrows[...] = jnp.dot(dispatch[...], en[...], preferred_element_type=f32).astype(bf16)

    pl.semaphore_wait(barrier, NZ * NX - 1 + NY - 1 + 1)

    mine = pl.multiple_of((z * NX + x) * CAP, CAP)
    for p, dzs in enumerate(NEAR):
        for dxs in range(NX):
            if dzs == 0 and dxs == 0:
                continue
            zt, xt = lax.rem(z + (NZ - dzs), NZ), lax.rem(x + (NX - dxs), NX)
            rcopy(
                outrows.at[pl.ds(pl.multiple_of((zt * NX + xt) * CAP, CAP), CAP)],
                xm.at[0, pl.ds((p * NX + dxs) * CAP, CAP)],
                ssem.at[1],
                dsem.at[p // 2],
                z=zt,
                x=xt,
            ).start()
    xm[0, 0:CAP, :] = outrows[pl.ds(mine, CAP), :]

    for cp in local[4:11]:
        cp.wait()
    dwcopy = rcopy(dw, dwp, ssem.at[0], msem.at[0], c=other)
    dwcopy.start()

    def norm_a(i, _):
        rows = pl.ds(pl.multiple_of(i * 16, 16), 16)
        v = mt[rows, :].astype(f32)
        sq = jnp.mean(v * v, axis=-1, keepdims=True)
        an[rows, :] = (v * lax.rsqrt(jnp.maximum(sq, MEAN_FLOOR)) * mg[...]).astype(bf16)
        return 0

    lax.fori_loop(0, ROWS_A // 16, norm_a, 0, unroll=4)
    w4[3 * HD : 4 * HD, :] = jnp.zeros((HD, D), bf16)
    pre = by_rows(fw[...], an[...]) + fb[...]
    log_gate = jnp.minimum(pre, 0.0) - jnp.log1p(jnp.exp(-jnp.abs(pre)))
    upto = (iota((ROWS_A, 256), 0) <= iota((ROWS_A, 256), 1)).astype(f32)
    gmb[...] = exact(jnp.broadcast_to(log_gate, (8, ROWS_A)), upto)
    for dx in range(1, NX):
        rcopy(gmb, gx.at[NX - dx], ssem.at[2], msem.at[1], x=lax.rem(x + dx, NX)).start()
    kvbuf[0:ROWS_A, :] = by_rows(an[...], w4[0 : 2 * HD, :]).astype(bf16)
    qs = by_rows(an[...], w4[2 * HD : 4 * HD, :]).astype(bf16) * jnp.asarray(HD**-0.5, bf16)
    qbuf[0:ROWS_A, :] = qs
    for dz in range(1, NZ):
        rcopy(
            kvbuf.at[pl.ds(0, ROWS_A)],
            kvbuf.at[pl.ds((NZ - dz) * ROWS_A, ROWS_A)],
            ssem.at[4],
            msem.at[3],
            z=lax.rem(z + dz, NZ),
        ).start()
    for dx in range(1, NX):
        rcopy(
            qbuf.at[pl.ds(0, ROWS_A)],
            qbuf.at[pl.ds((NX - dx) * ROWS_A, ROWS_A)],
            ssem.at[3],
            msem.at[2],
            x=lax.rem(x + dx, NX),
        ).start()

    up, down = lax.rem(y + 1, NY), lax.rem(y + NY - 1, NY)
    for g in range(4):
        skip = CAP if g == 0 else 0
        got = xm.at[0, pl.ds(g * 128 + skip, 128 - skip)]
        rcopy(got, got, ssem.at[1], dsem.at[g], c=other).wait_recv()
        piece = pl.ds(g * 128, 128)
        src = xm.at[0, piece]
        rcopy(src, xm.at[3, piece], ssem.at[6], ysem.at[3, g // 2], y=up).start()
        rcopy(src, xm.at[1, piece], ssem.at[7], ysem.at[1, g // 2], y=down).start()
        rcopy(src, xo.at[0, piece], ssem.at[9], psem.at[0], c=other).start()

    gx0 = gx.at[pl.ds(1, NX - 1)]
    rcopy(gx0, gx0, ssem.at[2], msem.at[1], x=x).wait_recv()
    ahead = jnp.zeros((8, 1), f32)
    total = gmb[:, 255:256]
    for k in range(1, NX):
        t = gx[k, :, 255:256]
        ahead = ahead + t * (lax.rem(x + k, NX) < x).astype(f32)
        total = total + t
    gadj[...] = jnp.where(iota((8, 256), 1) < ROWS_A, gmb[...] + ahead, total)
    for dz in range(1, NZ):
        rcopy(gadj, gz.at[NZ - dz], ssem.at[5], msem.at[4], z=lax.rem(z + dz, NZ)).start()

    for cp in local[11:]:
        cp.wait()

    def product(rows, k, core, start):
        cols = pl.ds(pl.multiple_of((lax.rem(y + k, 4) * 2 + core) * QUART, QUART), QUART)
        g, u = by_rows(rows, gw[:, cols]), by_rows(rows, uw[:, cols])
        if start:
            gacc[...], uacc[...] = g, u
        else:
            gacc[...] += g
            uacc[...] += u

    def arrived(k, h):
        half = xm.at[k, pl.ds(h * 256, 256)]
        rcopy(half, half, ssem.at[6], ysem.at[k, h], y=up).wait_recv()

    def to_partner(k):
        rcopy(xm.at[k], xo.at[k], ssem.at[10 + k], psem.at[k], c=other).start()

    def partner_product(k):
        rcopy(xo.at[k], xo.at[k], ssem.at[9], psem.at[k], c=other).wait_recv()
        product(xo[k], k, other, False)

    def relay(h):
        rows = pl.ds(h * 256, 256)
        arrived(3, h)
        src, dst = xm.at[3, rows, pl.ds(0, 128)], xm.at[2, rows, pl.ds(0, 128)]
        rcopy(src, dst, ssem.at[8], ysem.at[2, 0], y=up).start()
        arrived(1, h)
        src, dst = xm.at[1, rows, pl.ds(128, 128)], xm.at[2, rows, pl.ds(128, 128)]
        rcopy(src, dst, ssem.at[8], ysem.at[2, 0], y=down).start()

    product(xm[0], 0, c, True)
    relay(0)
    partner_product(0)
    relay(1)
    to_partner(3)
    to_partner(1)
    product(xm[3], 3, c, False)
    product(xm[1], 1, c, False)
    partner_product(3)
    partner_product(1)
    rcopy(xm.at[2], xm.at[2], ssem.at[6], ysem.at[2, 0], y=up).wait_recv()
    to_partner(2)
    product(xm[2], 2, c, False)
    partner_product(2)
    for h in range(2):
        rows = pl.ds(h * 256, 256)
        gate = gacc[rows, :]
        hid[rows, :] = (gate * jax.nn.sigmoid(gate) * uacc[rows, :]).astype(bf16)
        rcopy(hid.at[rows], hidp.at[rows], ssem.at[14], msem.at[6], c=other).start()

    def block(j, rows, weights):
        cols = pl.ds(pl.multiple_of((lax.rem(y + j, NY) * 2 + c) * 128, 128), 128)
        return jnp.dot(rows, weights[:, cols], preferred_element_type=f32)

    for j in (4, 3, 5, 2, 6, 1, 7, 0):
        pb[j] = block(j, hid[...], dw)
    dwcopy.wait_recv()
    rcopy(hid, hidp, ssem.at[14], msem.at[6], c=other).wait_recv()

    def plus(d, q, received):
        rows = pl.ds(q * 128, 128)
        v = pb[d, rows, :]
        if received:
            slot = rbp.at[d, rows]
            rcopy(slot, slot, ssem.at[15], rsp.at[d, q], y=up).wait_recv()
            v = v + rbp[d, rows, :].astype(f32)
        held = pl.ds(d * SLOTS + q * 128, 128)
        sbp[held, :] = v.astype(bf16)
        rcopy(
            sbp.at[held], rbp.at[d - 1, rows], ssem.at[15], rsp.at[d - 1, q], y=up
        ).start()

    def minus(d, q, received):
        rows = pl.ds(q * 128, 128)
        v = pb[NY - d, rows, :]
        if received:
            slot = rbm.at[d, rows]
            rcopy(slot, slot, ssem.at[16], rsm.at[d, q], y=down).wait_recv()
            v = v + rbm[d, rows, :].astype(f32)
        held = pl.ds(d * SLOTS + q * 128, 128)
        sbm[held, :] = v.astype(bf16)
        rcopy(
            sbm.at[held], rbm.at[d - 1, rows], ssem.at[16], rsm.at[d - 1, q], y=down
        ).start()

    HALF = ROWS_A // 2

    def attend(dx, half):
        rows = pl.ds(dx * ROWS_A + half * HALF, HALF)
        delta = (lax.rem(x + dx, NX) - x) * ROWS_A + half * HALF
        scores = by_rows(qbuf[rows, :], kvbuf[...]) + bias[0:1, :]
        lane = iota((HALF, 256), 1)
        seen = (lane <= iota((HALF, 256), 0) + delta) | (lane >= ROWS_A)
        scores = jnp.concatenate(
            [jnp.where(seen, scores[:, :256], LOW), scores[:, 256:]], axis=1
        )
        top = jnp.max(scores, axis=-1, keepdims=True)
        weight = jnp.exp(scores - top).astype(bf16)
        out = jnp.dot(weight, kvbuf[...], preferred_element_type=f32)
        po[rows, :] = jnp.where(iota((HALF, 128), 1) < HD, top, out)
        if half and dx:
            rcopy(
                po.at[pl.ds(dx * ROWS_A, ROWS_A)],
                pr.at[pl.ds((NX - dx) * ROWS_A, ROWS_A)],
                ssem.at[10],
                msem.at[5],
                x=lax.rem(x + dx, NX),
            ).start()

    pb[4] += block(4, hidp[...], dwp)
    for q in (0, 1):
        plus(4, q, False)
        minus(4, q + 2, False)
    for j in (3, 5):
        pb[j] += block(j, hidp[...], dwp)
    for q in (0, 1):
        plus(3, q + 2, False)
        minus(3, q, False)
    for j in (2, 6, 1, 7, 0):
        pb[j] += block(j, hidp[...], dwp)
    for q in (0, 1):
        plus(3, q, True)
        minus(3, q + 2, True)
    gz0 = gz.at[pl.ds(1, NZ - 1)]
    rcopy(gz0, gz0, ssem.at[5], msem.at[4], z=z).wait_recv()
    bias[:, 0:ROWS_A] = -gadj[:, 0:ROWS_A]
    back = jnp.zeros((8, 1), f32)
    for k in range(1, NZ):
        at = NZ - k
        back = back + gz[at, :, 255:256]
        bias[:, at * ROWS_A : (at + 1) * ROWS_A] = jnp.where(
            z - k >= 0, back - gz[at, :, 0:ROWS_A], LOW
        )
    q0 = qbuf.at[pl.ds(0, 3 * ROWS_A)]
    rcopy(q0, q0, ssem.at[3], msem.at[2], x=x).wait_recv()
    kv0 = kvbuf.at[pl.ds(0, 7 * ROWS_A)]
    rcopy(kv0, kv0, ssem.at[4], msem.at[3], z=z).wait_recv()
    order = [(2, 0), (2, 1), (1, 0), (1, 1), (3, 0), (3, 1), (0, 0), (0, 1)]
    for d in (2, 1):
        for q in (2, 3, 0, 1):
            plus(d, q, True)
            minus(d, (q + 2) % 4, True)
            attend(*order.pop(0))

    for q in (2, 0, 3, 1):
        rows = pl.ds(q * 128, 128)
        ps, ms = rbp.at[0, rows], rbm.at[0, rows]
        rcopy(ps, ps, ssem.at[15], rsp.at[0, q], y=up).wait_recv()
        rcopy(ms, ms, ssem.at[16], rsm.at[0, q], y=down).wait_recv()
        v = pb[0, rows, :] + rbp[0, rows, :].astype(f32) + rbm[0, rows, :].astype(f32)
        fin[rows, :] = v.astype(bf16)
        for p in (2 * q, 2 * q + 1):
            for dxs in range(NX):
                at = pl.ds((p * NX + dxs) * CAP, CAP)
                if p == 0 and dxs == 0:
                    res[pl.ds(mine, CAP), :] = fin[0:CAP, :]
                    continue
                rcopy(
                    fin.at[at],
                    res.at[pl.ds(mine, CAP)],
                    ssem.at[18],
                    msem.at[8],
                    z=lax.rem(z + NEAR[p], NZ),
                    x=lax.rem(x + dxs, NX),
                ).start()

    pr0 = pr.at[pl.ds(0, 3 * ROWS_A)]
    rcopy(pr0, pr0, ssem.at[10], msem.at[5], x=x).wait_recv()
    parts = [po[0:ROWS_A, :]] + [pr[k * ROWS_A : (k + 1) * ROWS_A, :] for k in range(1, NX)]
    tops = [p[:, 0:1] for p in parts]
    top = jnp.maximum(jnp.maximum(tops[0], tops[1]), jnp.maximum(tops[2], tops[3]))
    att = sum(p * jnp.exp(t - top) for p, t in zip(parts, tops))
    att = jnp.where(iota((ROWS_A, 128), 1) < HD, 0.0, att)
    mean = jnp.sum(att * att, axis=-1, keepdims=True) * (1.0 / HD)
    head = att * lax.rsqrt(mean + HEAD_FLOOR)
    packed = jnp.where(
        iota((HALF, 128), 1) < HD, pltpu.roll(head[:HALF], HD, 1), head[HALF:]
    )
    hbm[pl.ds(y, 1)] = packed.astype(bf16)[None]
    for dy in (4, 3, 5, 2, 6, 1, 7):
        rcopy(hbm.at[y], hbm.at[y], ssem.at[17], msem.at[7], y=lax.rem(y + dy, NY)).start()

    weights = first * rw[0:1, :] + second * rw[1:2, :]
    spread = exact(pick, weights)
    comb[...] = jnp.where(dispatch[...] > 0.5, spread, 0.0).T
    bw[...] = jnp.zeros_like(bw)
    for h in range(16):
        bw[h * 128 : h * 128 + HD, 0:128] = ow[h * HD : (h + 1) * HD, :]
        bw[h * 128 + HD : h * 128 + 128, 128:256] = ow[h * HD : (h + 1) * HD, :]

    h0 = hbm.at[pl.ds(0, NY - 1)]
    rcopy(h0, h0, ssem.at[17], msem.at[7], y=up).wait_recv()
    hc = rcopy(hbm, hbo, ssem.at[19], msem.at[9], c=other)
    hc.start()
    acc = jnp.zeros((HALF, 256), f32)
    for k in range(NY):
        acc = acc + jnp.dot(
            hbm[k], bw[pl.ds(pl.multiple_of((2 * k + c) * 128, 128), 128), :],
            preferred_element_type=f32,
        )

    r0 = res.at[pl.ds(0, SLOTS - CAP)]
    rcopy(r0, r0, ssem.at[18], msem.at[8], z=z).wait_recv()
    eo[...] = exact(comb[...], res[...].astype(f32)).astype(bf16)

    hc.wait_recv()
    for k in range(NY):
        acc = acc + jnp.dot(
            hbo[k], bw[pl.ds(pl.multiple_of((2 * k + other) * 128, 128), 128), :],
            preferred_element_type=f32,
        )
    mo[0:HALF, :] = acc[:, 0:128].astype(bf16)
    mo[HALF:ROWS_A, :] = acc[:, 128:256].astype(bf16)

    def sent(ref, sem):
        rcopy(ref, ref, ssem.at[sem], msem.at[0], c=other).wait_send()

    sent(dw, 0)
    sent(outrows.at[pl.ds(0, SLOTS - CAP)], 1)
    sent(gx0, 2)
    sent(q0, 3)
    sent(kv0, 4)
    sent(gz0, 5)
    for s in (6, 7, 8, 9):
        sent(xm.at[0], s)
    sent(pr0, 10)
    for s in (11, 12, 13):
        sent(xm.at[0], s)
    sent(hid, 14)
    for s in (15, 16):
        sent(sbp.at[pl.ds(0, 14 * 128)], s)
    sent(h0, 17)
    sent(r0, 18)
    sent(hbm, 19)


def on_device(mt, mg, qw, kw, vw, fw, fb, ow, et, eg, rt, rw, gw, uw, dw):
    vmem = pl.BlockSpec(memory_space=pltpu.VMEM)
    hbm = pl.BlockSpec(memory_space=pl.ANY)
    dma = pltpu.SemaphoreType.DMA
    return pl.pallas_call(
        kernel,
        name="mixer_and_experts",
        out_shape=(
            pltpu.VMEM((ROWS_A, 128), bf16),
            pltpu.VMEM((ROWS_B, 128), bf16),
        ),
        in_specs=[hbm] * 6 + [vmem] + [hbm] * 8,
        out_specs=(vmem, vmem),
        scratch_shapes=[
            pltpu.VMEM((ROWS_A, D), bf16),
            pltpu.VMEM((1, D), f32),
            pltpu.VMEM((1, D), bf16),
            pltpu.VMEM((16 * HD, 128), bf16),
            pltpu.VMEM((ROWS_B, D), bf16),
            pltpu.VMEM((1, D), f32),
            pltpu.VMEM((2, ROWS_B), jnp.int32),
            pltpu.VMEM((2, ROWS_B), f32),
            pltpu.VMEM((FF, D), bf16),
            pltpu.VMEM((FF, D), bf16),
            pltpu.VMEM((FF, D), bf16),
            pltpu.VMEM((FF, D), bf16),
            pltpu.VMEM((4 * HD, D), bf16),
            pltpu.VMEM((ROWS_A, D), bf16),
            pltpu.VMEM((ROWS_B, QUART), bf16),
            pltpu.VMEM((SLOTS, QUART), bf16),
            pltpu.VMEM((SLOTS, ROWS_B), bf16),
            pltpu.VMEM((ROWS_B, SLOTS), f32),
            pltpu.VMEM((4, SLOTS, QUART), bf16),
            pltpu.VMEM((4, SLOTS, QUART), bf16),
            pltpu.VMEM((SLOTS, FF), f32),
            pltpu.VMEM((SLOTS, FF), f32),
            pltpu.VMEM((SLOTS, FF), bf16),
            pltpu.VMEM((SLOTS, FF), bf16),
            pltpu.VMEM((NY, SLOTS, 128), f32),
            pltpu.VMEM((5 * SLOTS, 128), bf16),
            pltpu.VMEM((5 * SLOTS, 128), bf16),
            pltpu.VMEM((4, SLOTS, 128), bf16),
            pltpu.VMEM((4, SLOTS, 128), bf16),
            pltpu.VMEM((SLOTS, 128), bf16),
            pltpu.VMEM((SLOTS, 128), bf16),
            pltpu.VMEM((NX * ROWS_A, 128), bf16),
            pltpu.VMEM((NZ * ROWS_A, 128), bf16),
            pltpu.VMEM((8, 256), f32),
            pltpu.VMEM((NX, 8, 256), f32),
            pltpu.VMEM((8, 256), f32),
            pltpu.VMEM((NZ, 8, 256), f32),
            pltpu.VMEM((8, NZ * ROWS_A), f32),
            pltpu.VMEM((NX * ROWS_A, 128), f32),
            pltpu.VMEM((NX * ROWS_A, 128), f32),
            pltpu.VMEM((NY, ROWS_A // 2, 128), bf16),
            pltpu.VMEM((NY, ROWS_A // 2, 128), bf16),
            pltpu.VMEM((D, 256), bf16),
            dma((14,)),
            dma((20,)),
            dma((4,)),
            dma((4, 2)),
            dma((4,)),
            dma((4, 4)),
            dma((4, 4)),
            dma((10,)),
        ],
        compiler_params=pltpu.CompilerParams(collective_id=0, has_side_effects=True),
        cost_estimate=pl.CostEstimate(
            flops=3_000_000_000, bytes_accessed=6_000_000, transcendentals=1_200_000
        ),
    )(
        mt, mg.reshape(1, D), qw, kw, vw, fw.T, fb, ow, et, eg.reshape(1, D), rt.T, rw.T,
        gw, uw, dw,
    )


def solution(mesh):
    split = Mesh(mesh.devices.reshape(NZ, NX, NY, NC), ("z", "x", "y", "c"))
    return jax.shard_map(
        on_device,
        mesh=split,
        in_specs=(
            P(EP, None),
            P(),
            P(TP, None),
            P(TP, None),
            P(TP, None),
            P(None, TP),
            P(EP, TP),
            P(None, TP),
            P(EP, None),
            P(),
            P(EP, None),
            P(EP, None),
            P(EP, TP, None),
            P(EP, TP, None),
            P(EP, TP, None),
        ),
        out_specs=(P(EP, TP), P(EP, TP)),
        check_vma=False,
    )
```

time: 70.1 us -> 64.5 us (0.920)
  Pallas kernels: 66.6 us -> 61.5 us
  local copies, waits for them, and re-layouts: 2.05 us -> 1.24 us
    pallas_call x1, Pallas kernels: 66.6 us -> 61.5 us  [on_device(): pl.pallas_call(kernel, name='mixer_and_experts', out_shape=(pltpu.VMEM((R...]
    unnamed x4 -> x2, local copies, waits for them, and re-layouts: 2.05 us -> 1.24 us
where the time goes in v2:
time: 64.5 us; the launch traced here: 64 us
  Pallas kernels  61.5 us (95%)
  between operations  1.29 us (2%)
  local copies, waits for them, and re-layouts  1.24 us (2%)
    pallas_call x1, Pallas kernels, on_device(): pl.pallas_call(kernel, name='mixer_and_experts', out_shape=(pltpu.VMEM((R...  61.5 us

profile of v2, /device:TPU:1, one launch (start us, length us, event | category | flops | bytes accessed | tf_op | source)
XLA Modules:
  0.0 64.0 jit_solution(11301971715337568366)
XLA Ops:
  1.3 61.5 %mixer_and_experts.1 = (bf16[192,128]{1,0:T(8,128)(2,1)S(1)}, bf16[128,128]{1,0:T(8,128)(2,1)S(1)}) custom-call(bf16[192,2048]{1,0:T(8,128)(2,1)} %mt_h.1, f32[1,2048]{1,0:T(1,128)} %bitcast.5, bf16[64,2048]{1,0:T(8,128)(2,1)} %qw_h.1, bf16[64,2048]{1,0:T(8,128)(2,1)} %kw_h.1, bf16[64,2048]{1,0:T(8,128)(2,1)} %vw_h.1, bf16[1,2048]{1,0:T(2,128)(2,1)} %bitcast.6, ...), custom_call_target="tpu_custom_call" | custom-call | flops 3000000000 | bytes 6000000 | tf_op jit(solution)/shard_map/mixer_and_experts/pallas_call | solution.py:455
  62.8 0.6 copy.19
  63.4 0.6 copy.20

commit v3 on v2

--- a/solution.py
+++ b/solution.py
@@ -13,6 +13,8 @@
 D = 2048
 FF = 224
 CAP = 16
+HALF = ROWS_A // 2
+PIECE = (128, 128)
 SLOTS = NZ * NX * CAP
 QUART = 256
 MEAN_FLOOR = 0.1
@@ -49,13 +51,13 @@
 
 
 def kernel(
-    mt_h, mg_h, qw_h, kw_h, vw_h, fw_h, fb, ow_h, et_h, eg_h, rt_h, rw_h, gw_h, uw_h, dw_h,
+    mt_h, mg_h, qw_h, kw_h, vw_h, fw_h, fb_h, ow_h, et_h, eg_h, rt_h, rw_h, gw_h, uw_h, dw_h,
     mo, eo,
-    mt, mg, fw, ow, et, eg, rt, rw,
+    mt, mg, fw, fb, ow, et, eg, rt, rw,
     gw, uw, dw, dwp, w4, an, en, outrows, dispatch, comb,
     xm, xo, gacc, uacc, hid, hidp, pb, sbp, sbm, rbp, rbm, fin, res,
-    qbuf, kvbuf, gmb, gx, gadj, gz, bias, po, pr, hbm, hbo, bw,
-    lsem, ssem, dsem, ysem, psem, rsp, rsm, msem,
+    qbuf, kvbuf, gmb, gx, gadj, gz, bias, sc, wt, po, pr, hbm, hbo, bw,
+    lsem, ssem, dsem, ysem, psem, rsp, rsm, hsem, msem,
 ):
     z, x, y, c = (lax.axis_index(n) for n in ("z", "x", "y", "c"))
     other = 1 - c
@@ -74,6 +76,7 @@
                 (vw_h, w4.at[pl.ds(HD, HD)]),
                 (qw_h, w4.at[pl.ds(2 * HD, HD)]),
                 (fw_h, fw),
+                (fb_h, fb),
                 (dw_h.at[0], dw),
                 (gw_h.at[0], gw),
                 (uw_h.at[0], uw),
@@ -147,7 +150,7 @@
             ).start()
     xm[0, 0:CAP, :] = outrows[pl.ds(mine, CAP), :]
 
-    for cp in local[4:11]:
+    for cp in local[4:12]:
         cp.wait()
     dwcopy = rcopy(dw, dwp, ssem.at[0], msem.at[0], c=other)
     dwcopy.start()
@@ -170,14 +173,6 @@
     kvbuf[0:ROWS_A, :] = by_rows(an[...], w4[0 : 2 * HD, :]).astype(bf16)
     qs = by_rows(an[...], w4[2 * HD : 4 * HD, :]).astype(bf16) * jnp.asarray(HD**-0.5, bf16)
     qbuf[0:ROWS_A, :] = qs
-    for dz in range(1, NZ):
-        rcopy(
-            kvbuf.at[pl.ds(0, ROWS_A)],
-            kvbuf.at[pl.ds((NZ - dz) * ROWS_A, ROWS_A)],
-            ssem.at[4],
-            msem.at[3],
-            z=lax.rem(z + dz, NZ),
-        ).start()
     for dx in range(1, NX):
         rcopy(
             qbuf.at[pl.ds(0, ROWS_A)],
@@ -188,15 +183,97 @@
         ).start()
 
     up, down = lax.rem(y + 1, NY), lax.rem(y + NY - 1, NY)
-    for g in range(4):
+
+    def spread_own(g):
         skip = CAP if g == 0 else 0
         got = xm.at[0, pl.ds(g * 128 + skip, 128 - skip)]
         rcopy(got, got, ssem.at[1], dsem.at[g], c=other).wait_recv()
         piece = pl.ds(g * 128, 128)
         src = xm.at[0, piece]
-        rcopy(src, xm.at[3, piece], ssem.at[6], ysem.at[3, g // 2], y=up).start()
-        rcopy(src, xm.at[1, piece], ssem.at[7], ysem.at[1, g // 2], y=down).start()
-        rcopy(src, xo.at[0, piece], ssem.at[9], psem.at[0], c=other).start()
+        rcopy(src, xm.at[3, piece], ssem.at[6], ysem.at[3, g], y=up).start()
+        rcopy(src, xm.at[1, piece], ssem.at[7], ysem.at[1, g], y=down).start()
+        rcopy(src, xo.at[0, piece], ssem.at[9], psem.at[0, g // 2], c=other).start()
+
+    def product(h, src, k, core, start=False):
+        rows = pl.ds(h * 256, 256)
+        cols = pl.ds(pl.multiple_of((lax.rem(y + k, 4) * 2 + core) * QUART, QUART), QUART)
+        v = src[k, rows, :]
+        g, u = by_rows(v, gw[:, cols]), by_rows(v, uw[:, cols])
+        if start:
+            gacc[rows, :], uacc[rows, :] = g, u
+        else:
+            gacc[rows, :] += g
+            uacc[rows, :] += u
+
+    def arrived(k, g):
+        piece = xm.at[k, pl.ds(g * 128, 128)]
+        rcopy(piece, piece, ssem.at[6], ysem.at[k, g], y=up).wait_recv()
+
+    def to_partner(k, at, count):
+        rows = pl.ds(at, count)
+        rcopy(
+            xm.at[k, rows], xo.at[k, rows], ssem.at[10 + k], psem.at[k, at // 256], c=other
+        ).start()
+
+    def partner_product(h, k):
+        got = xo.at[k, pl.ds(h * 256, 256)]
+        rcopy(got, got, ssem.at[9], psem.at[k, h], c=other).wait_recv()
+        product(h, xo, k, other)
+
+    def relay(g):
+        rows = pl.ds(g * 128, 128)
+        for k, lane, to in ((3, 0, up), (1, 128, down)):
+            arrived(k, g)
+            rcopy(
+                xm.at[k, rows, pl.ds(lane, 128)],
+                xm.at[2, rows, pl.ds(lane, 128)],
+                ssem.at[8],
+                ysem.at[2, g],
+                y=to,
+            ).start()
+            to_partner(k, g * 128, 128)
+
+    def last_quarter(h):
+        arrived(2, 2 * h)
+        arrived(2, 2 * h + 1)
+        to_partner(2, h * 256, 256)
+        product(h, xm, 2, c)
+
+    def block(j, rows, weights):
+        cols = pl.ds(pl.multiple_of((lax.rem(y + j, NY) * 2 + c) * 128, 128), 128)
+        return jnp.dot(rows, weights[:, cols], preferred_element_type=f32)
+
+    BLOCKS = (4, 3, 5, 2, 6, 1, 7, 0)
+
+    def hidden(h):
+        partner_product(h, 2)
+        rows = pl.ds(h * 256, 256)
+        gate = gacc[rows, :]
+        hid[rows, :] = (gate * jax.nn.sigmoid(gate) * uacc[rows, :]).astype(bf16)
+        rcopy(hid.at[rows], hidp.at[rows], ssem.at[14], hsem.at[h], c=other).start()
+
+    def own_blocks(h):
+        rows = pl.ds(h * 256, 256)
+        for j in BLOCKS:
+            pb[j, rows, :] = block(j, hid[rows, :], dw)
+
+    def hidden_arrived(h):
+        got = hidp.at[pl.ds(h * 256, 256)]
+        rcopy(got, got, ssem.at[14], hsem.at[h], c=other).wait_recv()
+
+    def partner_blocks(h, which):
+        rows = pl.ds(h * 256, 256)
+        for j in which:
+            pb[j, rows, :] += block(j, hidp[rows, :], dwp)
+
+    spread_own(0)
+    spread_own(1)
+    for cp in local[12:]:
+        cp.wait()
+    product(0, xm, 0, c, True)
+    spread_own(2)
+    relay(0)
+    spread_own(3)
 
     gx0 = gx.at[pl.ds(1, NX - 1)]
     rcopy(gx0, gx0, ssem.at[2], msem.at[1], x=x).wait_recv()
@@ -209,110 +286,81 @@
     gadj[...] = jnp.where(iota((8, 256), 1) < ROWS_A, gmb[...] + ahead, total)
     for dz in range(1, NZ):
         rcopy(gadj, gz.at[NZ - dz], ssem.at[5], msem.at[4], z=lax.rem(z + dz, NZ)).start()
-
-    for cp in local[11:]:
-        cp.wait()
-
-    def product(rows, k, core, start):
-        cols = pl.ds(pl.multiple_of((lax.rem(y + k, 4) * 2 + core) * QUART, QUART), QUART)
-        g, u = by_rows(rows, gw[:, cols]), by_rows(rows, uw[:, cols])
-        if start:
-            gacc[...], uacc[...] = g, u
-        else:
-            gacc[...] += g
-            uacc[...] += u
-
-    def arrived(k, h):
-        half = xm.at[k, pl.ds(h * 256, 256)]
-        rcopy(half, half, ssem.at[6], ysem.at[k, h], y=up).wait_recv()
-
-    def to_partner(k):
-        rcopy(xm.at[k], xo.at[k], ssem.at[10 + k], psem.at[k], c=other).start()
-
-    def partner_product(k):
-        rcopy(xo.at[k], xo.at[k], ssem.at[9], psem.at[k], c=other).wait_recv()
-        product(xo[k], k, other, False)
-
-    def relay(h):
-        rows = pl.ds(h * 256, 256)
-        arrived(3, h)
-        src, dst = xm.at[3, rows, pl.ds(0, 128)], xm.at[2, rows, pl.ds(0, 128)]
-        rcopy(src, dst, ssem.at[8], ysem.at[2, 0], y=up).start()
-        arrived(1, h)
-        src, dst = xm.at[1, rows, pl.ds(128, 128)], xm.at[2, rows, pl.ds(128, 128)]
-        rcopy(src, dst, ssem.at[8], ysem.at[2, 0], y=down).start()
-
-    product(xm[0], 0, c, True)
-    relay(0)
-    partner_product(0)
+    for dz in range(1, NZ):
+        rcopy(
+            kvbuf.at[pl.ds(0, ROWS_A)],
+            kvbuf.at[pl.ds((NZ - dz) * ROWS_A, ROWS_A)],
+            ssem.at[4],
+            msem.at[3],
+            z=lax.rem(z + dz, NZ),
+        ).start()
+
     relay(1)
-    to_partner(3)
-    to_partner(1)
-    product(xm[3], 3, c, False)
-    product(xm[1], 1, c, False)
-    partner_product(3)
-    partner_product(1)
-    rcopy(xm.at[2], xm.at[2], ssem.at[6], ysem.at[2, 0], y=up).wait_recv()
-    to_partner(2)
-    product(xm[2], 2, c, False)
-    partner_product(2)
-    for h in range(2):
-        rows = pl.ds(h * 256, 256)
-        gate = gacc[rows, :]
-        hid[rows, :] = (gate * jax.nn.sigmoid(gate) * uacc[rows, :]).astype(bf16)
-        rcopy(hid.at[rows], hidp.at[rows], ssem.at[14], msem.at[6], c=other).start()
-
-    def block(j, rows, weights):
-        cols = pl.ds(pl.multiple_of((lax.rem(y + j, NY) * 2 + c) * 128, 128), 128)
-        return jnp.dot(rows, weights[:, cols], preferred_element_type=f32)
-
-    for j in (4, 3, 5, 2, 6, 1, 7, 0):
-        pb[j] = block(j, hid[...], dw)
+    product(1, xm, 0, c, True)
+    partner_product(0, 0)
+    product(0, xm, 3, c)
+    relay(2)
+    product(0, xm, 1, c)
+    partner_product(0, 3)
+    partner_product(0, 1)
+    relay(3)
+    partner_product(1, 0)
+    last_quarter(0)
+    product(1, xm, 3, c)
+    product(1, xm, 1, c)
+    hidden(0)
+    partner_product(1, 3)
+    partner_product(1, 1)
+    own_blocks(0)
     dwcopy.wait_recv()
-    rcopy(hid, hidp, ssem.at[14], msem.at[6], c=other).wait_recv()
-
-    def plus(d, q, received):
-        rows = pl.ds(q * 128, 128)
-        v = pb[d, rows, :]
+
+    def onward(d, at, count, received, way):
+        got, out, recv, to, sem, j = (
+            (rbp, sbp, rsp, up, 15, d) if way else (rbm, sbm, rsm, down, 16, NY - d)
+        )
+        rows = pl.ds(at, count)
+        v = pb[j, rows, :]
         if received:
-            slot = rbp.at[d, rows]
-            rcopy(slot, slot, ssem.at[15], rsp.at[d, q], y=up).wait_recv()
-            v = v + rbp[d, rows, :].astype(f32)
-        held = pl.ds(d * SLOTS + q * 128, 128)
-        sbp[held, :] = v.astype(bf16)
+            slot = got.at[d, rows]
+            rcopy(slot, slot, ssem.at[sem], recv.at[d, at // 64], y=to).wait_recv()
+            v = v + got[d, rows, :].astype(f32)
+        held = pl.ds(d * SLOTS + at, count)
+        out[held, :] = v.astype(bf16)
         rcopy(
-            sbp.at[held], rbp.at[d - 1, rows], ssem.at[15], rsp.at[d - 1, q], y=up
+            out.at[held], got.at[d - 1, rows], ssem.at[sem], recv.at[d - 1, at // 64], y=to
         ).start()
 
-    def minus(d, q, received):
-        rows = pl.ds(q * 128, 128)
-        v = pb[NY - d, rows, :]
-        if received:
-            slot = rbm.at[d, rows]
-            rcopy(slot, slot, ssem.at[16], rsm.at[d, q], y=down).wait_recv()
-            v = v + rbm[d, rows, :].astype(f32)
-        held = pl.ds(d * SLOTS + q * 128, 128)
-        sbm[held, :] = v.astype(bf16)
-        rcopy(
-            sbm.at[held], rbm.at[d - 1, rows], ssem.at[16], rsm.at[d - 1, q], y=down
-        ).start()
-
-    HALF = ROWS_A // 2
-
-    def attend(dx, half):
-        rows = pl.ds(dx * ROWS_A + half * HALF, HALF)
-        delta = (lax.rem(x + dx, NX) - x) * ROWS_A + half * HALF
-        scores = by_rows(qbuf[rows, :], kvbuf[...]) + bias[0:1, :]
-        lane = iota((HALF, 256), 1)
-        seen = (lane <= iota((HALF, 256), 0) + delta) | (lane >= ROWS_A)
-        scores = jnp.concatenate(
-            [jnp.where(seen, scores[:, :256], LOW), scores[:, 256:]], axis=1
-        )
-        top = jnp.max(scores, axis=-1, keepdims=True)
-        weight = jnp.exp(scores - top).astype(bf16)
-        out = jnp.dot(weight, kvbuf[...], preferred_element_type=f32)
-        po[rows, :] = jnp.where(iota((HALF, 128), 1) < HD, top, out)
-        if half and dx:
+    def both(d, h, even, received):
+        for i in range(0, 128, PIECE[h]):
+            first = h * 256 + (0 if even else 128) + i
+            second = h * 256 + (128 if even else 0) + i
+            onward(d, first, PIECE[h], received, True)
+            onward(d, second, PIECE[h], received, False)
+
+    def scored(half):
+        rows = pl.ds(half * 2 * ROWS_A, 2 * ROWS_A)
+        sc[rows, :] = by_rows(qbuf[rows, :], kvbuf[...]) + bias[0:1, :]
+
+    def weighed(dx):
+        lane, row = iota((32, 256), 1), iota((32, 256), 0)
+        for i in range(ROWS_A // 32):
+            rows = pl.ds(dx * ROWS_A + i * 32, 32)
+            delta = (lax.rem(x + dx, NX) - x) * ROWS_A + i * 32
+            seen = (lane <= row + delta) | (lane >= ROWS_A)
+            near = jnp.where(seen, sc[rows, 0:256], LOW)
+            far = sc[rows, 256:]
+            top = jnp.maximum(
+                jnp.max(near, axis=-1, keepdims=True), jnp.max(far, axis=-1, keepdims=True)
+            )
+            wt[rows, 0:256] = jnp.exp(near - top).astype(bf16)
+            wt[rows, 256:] = jnp.exp(far - top).astype(bf16)
+            po[rows, :] = jnp.broadcast_to(top, (32, 128))
+
+    def summed(half):
+        rows = pl.ds(half * 2 * ROWS_A, 2 * ROWS_A)
+        out = jnp.dot(wt[rows, :], kvbuf[...], preferred_element_type=f32)
+        po[rows, :] = jnp.where(iota((2 * ROWS_A, 128), 1) < HD, po[rows, :], out)
+        for dx in (2, 3) if half else (1,):
             rcopy(
                 po.at[pl.ds(dx * ROWS_A, ROWS_A)],
                 pr.at[pl.ds((NX - dx) * ROWS_A, ROWS_A)],
@@ -321,20 +369,33 @@
                 x=lax.rem(x + dx, NX),
             ).start()
 
-    pb[4] += block(4, hidp[...], dwp)
-    for q in (0, 1):
-        plus(4, q, False)
-        minus(4, q + 2, False)
-    for j in (3, 5):
-        pb[j] += block(j, hidp[...], dwp)
-    for q in (0, 1):
-        plus(3, q + 2, False)
-        minus(3, q, False)
-    for j in (2, 6, 1, 7, 0):
-        pb[j] += block(j, hidp[...], dwp)
-    for q in (0, 1):
-        plus(3, q, True)
-        minus(3, q + 2, True)
+    steps = [
+        (scored, 1), (weighed, 2), (weighed, 3), (summed, 1),
+        (scored, 0), (weighed, 1), (weighed, 0), (summed, 0),
+    ]
+
+    def attend(count):
+        for _ in range(count):
+            step, arg = steps.pop(0)
+            step(arg)
+
+    hidden_arrived(0)
+    partner_blocks(0, (4,))
+    both(4, 0, True, False)
+    partner_blocks(0, (3, 5))
+    both(3, 0, False, False)
+    last_quarter(1)
+    partner_blocks(0, (2, 6, 1, 7, 0))
+    hidden(1)
+    own_blocks(1)
+    hidden_arrived(1)
+    partner_blocks(1, (4,))
+    both(4, 1, True, False)
+    partner_blocks(1, (3, 5))
+    both(3, 1, False, False)
+    both(3, 0, True, True)
+    both(2, 0, False, True)
+    partner_blocks(1, (2, 6, 1, 7, 0))
     gz0 = gz.at[pl.ds(1, NZ - 1)]
     rcopy(gz0, gz0, ssem.at[5], msem.at[4], z=z).wait_recv()
     bias[:, 0:ROWS_A] = -gadj[:, 0:ROWS_A]
@@ -349,18 +410,26 @@
     rcopy(q0, q0, ssem.at[3], msem.at[2], x=x).wait_recv()
     kv0 = kvbuf.at[pl.ds(0, 7 * ROWS_A)]
     rcopy(kv0, kv0, ssem.at[4], msem.at[3], z=z).wait_recv()
-    order = [(2, 0), (2, 1), (1, 0), (1, 1), (3, 0), (3, 1), (0, 0), (0, 1)]
-    for d in (2, 1):
-        for q in (2, 3, 0, 1):
-            plus(d, q, True)
-            minus(d, (q + 2) % 4, True)
-            attend(*order.pop(0))
-
-    for q in (2, 0, 3, 1):
+    attend(3)
+    both(3, 1, True, True)
+    both(2, 1, False, True)
+    attend(1)
+    both(2, 0, True, True)
+    both(1, 0, False, True)
+    attend(3)
+    both(2, 1, True, True)
+    both(1, 1, False, True)
+    attend(1)
+    both(1, 0, True, True)
+    both(1, 1, True, True)
+
+    def last(q):
         rows = pl.ds(q * 128, 128)
-        ps, ms = rbp.at[0, rows], rbm.at[0, rows]
-        rcopy(ps, ps, ssem.at[15], rsp.at[0, q], y=up).wait_recv()
-        rcopy(ms, ms, ssem.at[16], rsm.at[0, q], y=down).wait_recv()
+        piece = PIECE[q // 2]
+        for at in range(q * 128, q * 128 + 128, piece):
+            ps, ms = rbp.at[0, pl.ds(at, piece)], rbm.at[0, pl.ds(at, piece)]
+            rcopy(ps, ps, ssem.at[15], rsp.at[0, at // 64], y=up).wait_recv()
+            rcopy(ms, ms, ssem.at[16], rsm.at[0, at // 64], y=down).wait_recv()
         v = pb[0, rows, :] + rbp[0, rows, :].astype(f32) + rbm[0, rows, :].astype(f32)
         fin[rows, :] = v.astype(bf16)
         for p in (2 * q, 2 * q + 1):
@@ -378,6 +447,9 @@
                     x=lax.rem(x + dxs, NX),
                 ).start()
 
+    last(1)
+    last(0)
+
     pr0 = pr.at[pl.ds(0, 3 * ROWS_A)]
     rcopy(pr0, pr0, ssem.at[10], msem.at[5], x=x).wait_recv()
     parts = [po[0:ROWS_A, :]] + [pr[k * ROWS_A : (k + 1) * ROWS_A, :] for k in range(1, NX)]
@@ -394,9 +466,16 @@
     for dy in (4, 3, 5, 2, 6, 1, 7):
         rcopy(hbm.at[y], hbm.at[y], ssem.at[17], msem.at[7], y=lax.rem(y + dy, NY)).start()
 
+    last(3)
+    last(2)
+
     weights = first * rw[0:1, :] + second * rw[1:2, :]
     spread = exact(pick, weights)
-    comb[...] = jnp.where(dispatch[...] > 0.5, spread, 0.0).T
+    rest = jnp.where(dispatch[...] > 0.5, spread, 0.0).T
+    for k in range(3):
+        term = rest.astype(bf16)
+        comb[k] = term
+        rest = rest - term.astype(f32)
     bw[...] = jnp.zeros_like(bw)
     for h in range(16):
         bw[h * 128 : h * 128 + HD, 0:128] = ow[h * HD : (h + 1) * HD, :]
@@ -415,7 +494,9 @@
 
     r0 = res.at[pl.ds(0, SLOTS - CAP)]
     rcopy(r0, r0, ssem.at[18], msem.at[8], z=z).wait_recv()
-    eo[...] = exact(comb[...], res[...].astype(f32)).astype(bf16)
+    eo[...] = sum(
+        jnp.dot(comb[k], res[...], preferred_element_type=f32) for k in range(3)
+    ).astype(bf16)
 
     hc.wait_recv()
     for k in range(NY):
@@ -459,12 +540,13 @@
             pltpu.VMEM((ROWS_A, 128), bf16),
             pltpu.VMEM((ROWS_B, 128), bf16),
         ),
-        in_specs=[hbm] * 6 + [vmem] + [hbm] * 8,
+        in_specs=[hbm] * 15,
         out_specs=(vmem, vmem),
         scratch_shapes=[
             pltpu.VMEM((ROWS_A, D), bf16),
             pltpu.VMEM((1, D), f32),
             pltpu.VMEM((1, D), bf16),
+            pltpu.VMEM((1, 1), f32),
             pltpu.VMEM((16 * HD, 128), bf16),
             pltpu.VMEM((ROWS_B, D), bf16),
             pltpu.VMEM((1, D), f32),
@@ -479,7 +561,7 @@
             pltpu.VMEM((ROWS_B, QUART), bf16),
             pltpu.VMEM((SLOTS, QUART), bf16),
             pltpu.VMEM((SLOTS, ROWS_B), bf16),
-            pltpu.VMEM((ROWS_B, SLOTS), f32),
+            pltpu.VMEM((3, ROWS_B, SLOTS), bf16),
             pltpu.VMEM((4, SLOTS, QUART), bf16),
             pltpu.VMEM((4, SLOTS, QUART), bf16),
             pltpu.VMEM((SLOTS, FF), f32),
@@ -500,18 +582,21 @@
             pltpu.VMEM((8, 256), f32),
             pltpu.VMEM((NZ, 8, 256), f32),
             pltpu.VMEM((8, NZ * ROWS_A), f32),
+            pltpu.VMEM((NX * ROWS_A, NZ * ROWS_A), f32),
+            pltpu.VMEM((NX * ROWS_A, NZ * ROWS_A), bf16),
             pltpu.VMEM((NX * ROWS_A, 128), f32),
             pltpu.VMEM((NX * ROWS_A, 128), f32),
             pltpu.VMEM((NY, ROWS_A // 2, 128), bf16),
             pltpu.VMEM((NY, ROWS_A // 2, 128), bf16),
             pltpu.VMEM((D, 256), bf16),
-            dma((14,)),
+            dma((15,)),
             dma((20,)),
             dma((4,)),
+            dma((4, 4)),
             dma((4, 2)),
-            dma((4,)),
-            dma((4, 4)),
-            dma((4, 4)),
+            dma((4, 8)),
+            dma((4, 8)),
+            dma((2,)),
             dma((10,)),
         ],
         compiler_params=pltpu.CompilerParams(collective_id=0, has_side_effects=True),

time: 64.5 us -> 60.5 us (0.938)
  Pallas kernels: 61.5 us -> 57.9 us
    pallas_call x1, Pallas kernels: 61.5 us -> 57.9 us  [on_device(): pl.pallas_call(kernel, name='mixer_and_experts', out_shape=(pltpu.VMEM((R...]
where the time goes in v3:
time: 60.5 us; the launch traced here: 60.4 us
  Pallas kernels  57.9 us (96%)
  between operations  1.29 us (2%)
  local copies, waits for them, and re-layouts  1.24 us (2%)
    pallas_call x1, Pallas kernels, on_device(): pl.pallas_call(kernel, name='mixer_and_experts', out_shape=(pltpu.VMEM((R...  57.9 us
    unnamed x2, local copies, waits for them, and re-layouts  1.24 us

profile of v3, /device:TPU:1, one launch (start us, length us, event | category | flops | bytes accessed | tf_op | source)
XLA Modules:
  0.0 60.4 jit_solution(10919592128453216609)
XLA Ops:
  1.3 57.9 %mixer_and_experts.1 = (bf16[192,128]{1,0:T(8,128)(2,1)S(1)}, bf16[128,128]{1,0:T(8,128)(2,1)S(1)}) custom-call(bf16[192,2048]{1,0:T(8,128)(2,1)} %mt_h.1, f32[1,2048]{1,0:T(1,128)} %bitcast.5, bf16[64,2048]{1,0:T(8,128)(2,1)} %qw_h.1, bf16[64,2048]{1,0:T(8,128)(2,1)} %kw_h.1, bf16[64,2048]{1,0:T(8,128)(2,1)} %vw_h.1, bf16[1,2048]{1,0:T(2,128)(2,1)} %bitcast.6, ...), custom_call_target="tpu_custom_call" | custom-call | flops 3000000000 | bytes 6000000 | tf_op jit(solution)/shard_map/mixer_and_experts/pallas_call | solution.py:536
  59.2 0.6 %copy.19 = bf16[192,128]{1,0:T(8,128)(2,1)} copy(bf16[192,128]{1,0:T(8,128)(2,1)S(1)} %get-tuple-element.2) | data formatting | bytes 98304
  59.8 0.6 %copy.20 = bf16[128,128]{1,0:T(8,128)(2,1)} copy(bf16[128,128]{1,0:T(8,128)(2,1)S(1)} %get-tuple-element.3) | data formatting | bytes 65536

commit v4 on v3

--- a/solution.py
+++ b/solution.py
@@ -84,12 +84,12 @@
             )
         )
     ]
-    for cp in local[:4]:
+    for cp in (local[2], local[0], local[1], local[3]):
         cp.start()
 
     barrier = pltpu.get_barrier_semaphore()
-    for dz in range(NZ):
-        for dx in range(NX):
+    for dz in reversed(NEAR):
+        for dx in (2, 1, 3, 0):
             if dz or dx:
                 pl.semaphore_signal(
                     barrier,
@@ -97,7 +97,7 @@
                     device_id={"z": lax.rem(z + dz, NZ), "x": lax.rem(x + dx, NX)},
                     device_id_type=MESH,
                 )
-    for dy in range(1, NY):
+    for dy in NEAR[:0:-1]:
         pl.semaphore_signal(
             barrier, inc=1, device_id={"y": lax.rem(y + dy, NY)}, device_id_type=MESH
         )
@@ -108,8 +108,7 @@
     eid = iota((32, ROWS_B), 0)
     before = (iota((ROWS_B, ROWS_B), 0) < iota((ROWS_B, ROWS_B), 1)).astype(bf16)
     pick = (lax.div(iota((SLOTS, 32), 0), CAP) == iota((SLOTS, 32), 1)).astype(f32)
-    for cp in local[:4]:
-        cp.wait()
+    local[2].wait()
     first = (eid == rt[0:1, :]).astype(f32)
     second = (eid == rt[1:2, :]).astype(f32)
     named = first + second
@@ -118,6 +117,8 @@
     wide = jnp.dot(pick.astype(bf16), rank.astype(bf16), preferred_element_type=f32)
     chosen = wide == lax.rem(iota((SLOTS, ROWS_B), 0), CAP).astype(f32)
     dispatch[...] = chosen.astype(f32).astype(bf16)
+    for cp in (local[0], local[1], local[3]):
+        cp.wait()
     lane0 = pl.multiple_of((lax.rem(y, 4) * 2 + c) * QUART, QUART)
 
     def norm_b(i, _):
@@ -129,7 +130,7 @@
         en[rows, :] = scaled.astype(bf16)
         return 0
 
-    lax.fori_loop(0, ROWS_B // 16, norm_b, 0, unroll=4)
+    lax.fori_loop(0, ROWS_B // 16, norm_b, 0, unroll=8)
     outrows[...] = jnp.dot(dispatch[...], en[...], preferred_element_type=f32).astype(bf16)
 
     pl.semaphore_wait(barrier, NZ * NX - 1 + NY - 1 + 1)
@@ -291,7 +292,7 @@
             kvbuf.at[pl.ds(0, ROWS_A)],
             kvbuf.at[pl.ds((NZ - dz) * ROWS_A, ROWS_A)],
             ssem.at[4],
-            msem.at[3],
+            msem.at[10],
             z=lax.rem(z + dz, NZ),
         ).start()
 
@@ -409,7 +410,7 @@
     q0 = qbuf.at[pl.ds(0, 3 * ROWS_A)]
     rcopy(q0, q0, ssem.at[3], msem.at[2], x=x).wait_recv()
     kv0 = kvbuf.at[pl.ds(0, 7 * ROWS_A)]
-    rcopy(kv0, kv0, ssem.at[4], msem.at[3], z=z).wait_recv()
+    rcopy(kv0, kv0, ssem.at[4], msem.at[10], z=z).wait_recv()
     attend(3)
     both(3, 1, True, True)
     both(2, 1, False, True)
@@ -464,7 +465,13 @@
     )
     hbm[pl.ds(y, 1)] = packed.astype(bf16)[None]
     for dy in (4, 3, 5, 2, 6, 1, 7):
-        rcopy(hbm.at[y], hbm.at[y], ssem.at[17], msem.at[7], y=lax.rem(y + dy, NY)).start()
+        rcopy(
+            hbm.at[y],
+            hbm.at[y],
+            ssem.at[17],
+            msem.at[7 if dy in (3, 4, 5) else 3],
+            y=lax.rem(y + dy, NY),
+        ).start()
 
     last(3)
     last(2)
@@ -482,9 +489,13 @@
         bw[h * 128 + HD : h * 128 + 128, 128:256] = ow[h * HD : (h + 1) * HD, :]
 
     h0 = hbm.at[pl.ds(0, NY - 1)]
-    rcopy(h0, h0, ssem.at[17], msem.at[7], y=up).wait_recv()
     hc = rcopy(hbm, hbo, ssem.at[19], msem.at[9], c=other)
-    hc.start()
+    for sem, offsets in ((3, (0, 1, 7, 2, 6)), (7, (3, 5, 4))):
+        some = hbm.at[pl.ds(0, 4 if sem == 3 else 3)]
+        rcopy(some, some, ssem.at[17], msem.at[sem], y=up).wait_recv()
+        for dy in offsets:
+            at = lax.rem(y + dy, NY)
+            rcopy(hbm.at[at], hbo.at[at], ssem.at[19], msem.at[9], c=other).start()
     acc = jnp.zeros((HALF, 256), f32)
     for k in range(NY):
         acc = acc + jnp.dot(
@@ -493,19 +504,33 @@
         )
 
     r0 = res.at[pl.ds(0, SLOTS - CAP)]
-    rcopy(r0, r0, ssem.at[18], msem.at[8], z=z).wait_recv()
-    eo[...] = sum(
-        jnp.dot(comb[k], res[...], preferred_element_type=f32) for k in range(3)
-    ).astype(bf16)
-
-    hc.wait_recv()
-    for k in range(NY):
-        acc = acc + jnp.dot(
-            hbo[k], bw[pl.ds(pl.multiple_of((2 * k + other) * 128, 128), 128), :],
-            preferred_element_type=f32,
-        )
-    mo[0:HALF, :] = acc[:, 0:128].astype(bf16)
-    mo[HALF:ROWS_A, :] = acc[:, 128:256].astype(bf16)
+
+    def experts_out():
+        rcopy(r0, r0, ssem.at[18], msem.at[8], z=z).wait_recv()
+        eo[...] = sum(
+            jnp.dot(comb[k], res[...], preferred_element_type=f32) for k in range(3)
+        ).astype(bf16)
+
+    def mixer_out():
+        hc.wait_recv()
+        whole = acc
+        for k in range(NY):
+            whole = whole + jnp.dot(
+                hbo[k], bw[pl.ds(pl.multiple_of((2 * k + other) * 128, 128), 128), :],
+                preferred_element_type=f32,
+            )
+        mo[0:HALF, :] = whole[:, 0:128].astype(bf16)
+        mo[HALF:ROWS_A, :] = whole[:, 128:256].astype(bf16)
+
+    @pl.when(c == 0)
+    def _():
+        mixer_out()
+        experts_out()
+
+    @pl.when(c == 1)
+    def _():
+        experts_out()
+        mixer_out()
 
     def sent(ref, sem):
         rcopy(ref, ref, ssem.at[sem], msem.at[0], c=other).wait_send()
@@ -597,7 +622,7 @@
             dma((4, 8)),
             dma((4, 8)),
             dma((2,)),
-            dma((10,)),
+            dma((11,)),
         ],
         compiler_params=pltpu.CompilerParams(collective_id=0, has_side_effects=True),
         cost_estimate=pl.CostEstimate(

time: 60.5 us -> 59.8 us (0.988)
  Pallas kernels: 57.9 us -> 57.1 us
    pallas_call x1, Pallas kernels: 57.9 us -> 57.1 us  [on_device(): pl.pallas_call(kernel, name='mixer_and_experts', out_shape=(pltpu.VMEM((R...]
where the time goes in v4:
time: 59.8 us; the launch traced here: 59.6 us
  Pallas kernels  57.1 us (95%)
  between operations  1.29 us (2%)
  local copies, waits for them, and re-layouts  1.24 us (2%)
    pallas_call x1, Pallas kernels, on_device(): pl.pallas_call(kernel, name='mixer_and_experts', out_shape=(pltpu.VMEM((R...  57.1 us
    unnamed x2, local copies, waits for them, and re-layouts  1.24 us

profile of v4, /device:TPU:1, one launch (start us, length us, event | category | flops | bytes accessed | tf_op | source)
XLA Modules:
  0.0 59.6 jit_solution(2781461810956310758)
XLA Ops:
  1.3 57.1 %mixer_and_experts.1 = (bf16[192,128]{1,0:T(8,128)(2,1)S(1)}, bf16[128,128]{1,0:T(8,128)(2,1)S(1)}) custom-call(bf16[192,2048]{1,0:T(8,128)(2,1)} %mt_h.1, f32[1,2048]{1,0:T(1,128)} %bitcast.5, bf16[64,2048]{1,0:T(8,128)(2,1)} %qw_h.1, bf16[64,2048]{1,0:T(8,128)(2,1)} %kw_h.1, bf16[64,2048]{1,0:T(8,128)(2,1)} %vw_h.1, bf16[1,2048]{1,0:T(2,128)(2,1)} %bitcast.6, ...), custom_call_target="tpu_custom_call" | custom-call | flops 3000000000 | bytes 6000000 | tf_op jit(solution)/shard_map/mixer_and_experts/pallas_call | solution.py:561
  58.4 0.6 %copy.19 = bf16[192,128]{1,0:T(8,128)(2,1)} copy(bf16[192,128]{1,0:T(8,128)(2,1)S(1)} %get-tuple-element.2) | data formatting | bytes 98304
  59.0 0.6 %copy.20 = bf16[128,128]{1,0:T(8,128)(2,1)} copy(bf16[128,128]{1,0:T(8,128)(2,1)S(1)} %get-tuple-element.3) | data formatting | bytes 65536

commit v5 on v4

--- a/solution.py
+++ b/solution.py
@@ -23,7 +23,8 @@
 MESH = pl.DeviceIdType.MESH
 TP = ("y", "c")
 EP = ("z", "x")
-NEAR = (0, 1, 7, 2, 6, 3, 5, 4)
+NEAR = (0, 1, 5, 4, 3, 6, 2, 7)
+FAR_FIRST = (4, 3, 5, 2, 6, 1, 7, 0)
 f32, bf16 = jnp.float32, jnp.bfloat16
 
 
@@ -88,7 +89,7 @@
         cp.start()
 
     barrier = pltpu.get_barrier_semaphore()
-    for dz in reversed(NEAR):
+    for dz in FAR_FIRST:
         for dx in (2, 1, 3, 0):
             if dz or dx:
                 pl.semaphore_signal(
@@ -97,7 +98,7 @@
                     device_id={"z": lax.rem(z + dz, NZ), "x": lax.rem(x + dx, NX)},
                     device_id_type=MESH,
                 )
-    for dy in NEAR[:0:-1]:
+    for dy in FAR_FIRST[:-1]:
         pl.semaphore_signal(
             barrier, inc=1, device_id={"y": lax.rem(y + dy, NY)}, device_id_type=MESH
         )

time: 59.8 us -> 61.3 us (1.025)
  Pallas kernels: 57.1 us -> 58.7 us
    pallas_call x1, Pallas kernels: 57.1 us -> 58.7 us  [on_device(): pl.pallas_call(kernel, name='mixer_and_experts', out_shape=(pltpu.VMEM((R...]
where the time goes in v5:
time: 61.3 us; the launch traced here: 61.2 us
  Pallas kernels  58.7 us (96%)
  between operations  1.29 us (2%)
  local copies, waits for them, and re-layouts  1.24 us (2%)
    pallas_call x1, Pallas kernels, on_device(): pl.pallas_call(kernel, name='mixer_and_experts', out_shape=(pltpu.VMEM((R...  58.7 us
    unnamed x2, local copies, waits for them, and re-layouts  1.24 us

profile of v5, /device:TPU:1, one launch (start us, length us, event | category | flops | bytes accessed | tf_op | source)
XLA Modules:
  0.0 61.2 jit_solution(9374383767575461100)
XLA Ops:
  1.3 58.7 %mixer_and_experts.1 = (bf16[192,128]{1,0:T(8,128)(2,1)S(1)}, bf16[128,128]{1,0:T(8,128)(2,1)S(1)}) custom-call(bf16[192,2048]{1,0:T(8,128)(2,1)} %mt_h.1, f32[1,2048]{1,0:T(1,128)} %bitcast.5, bf16[64,2048]{1,0:T(8,128)(2,1)} %qw_h.1, bf16[64,2048]{1,0:T(8,128)(2,1)} %kw_h.1, bf16[64,2048]{1,0:T(8,128)(2,1)} %vw_h.1, bf16[1,2048]{1,0:T(2,128)(2,1)} %bitcast.6, ...), custom_call_target="tpu_custom_call" | custom-call | flops 3000000000 | bytes 6000000 | tf_op jit(solution)/shard_map/mixer_and_experts/pallas_call | solution.py:562
  59.9 0.6 %copy.19 = bf16[192,128]{1,0:T(8,128)(2,1)} copy(bf16[192,128]{1,0:T(8,128)(2,1)S(1)} %get-tuple-element.2) | data formatting | bytes 98304
  60.6 0.6 %copy.20 = bf16[128,128]{1,0:T(8,128)(2,1)} copy(bf16[128,128]{1,0:T(8,128)(2,1)S(1)} %get-tuple-element.3) | data formatting | bytes 65536
